TPU v7x, 256 devices: a whole 4x4x8 slice. The times are simulated.
256 devices in a mesh: ep: 64 (over z, x, core), tp: 4 (over y).
Axes of the slice: x: 4, y: 4, z: 8, core: 2. Of those that a mesh axis runs over, the one named last changes fastest.
Arguments:
- tokens: bfloat16 [1024, 2048], P('ep'), may hold values from -6 to 6
- attn_gain: float32 [2048], replicated, may hold values from 0.1 to 1.9
- query_weight: bfloat16 [2048, 2048], P('ep', 'tp'), may hold values from -0.125 to 0.125
- key_weight: bfloat16 [2048, 512], P('ep', 'tp'), may hold values from -0.125 to 0.125
- value_weight: bfloat16 [2048, 512], P('ep', 'tp'), may hold values from -0.125 to 0.125
- break_bias: float32 [16], P('tp'), may hold values from -14 to -8
- cache_keys: bfloat16 [1024, 4, 1024, 128], P('ep', 'tp'), may hold values from -18 to 18
- cache_values: bfloat16 [1024, 4, 1024, 128], P('ep', 'tp'), may hold values from -6 to 6
- lengths: int32 [1024], P('ep'), may hold values from 1 to 1024, 524288 in all
- out_weight: bfloat16 [2048, 2048], P('tp', 'ep'), may hold values from -0.25 to 0.25
- ffn_gain: float32 [2048], replicated, may hold values from 0.1 to 1.9
- branch_gate: bfloat16 [2048], replicated, may hold values from -0.125 to 0.125
- dense_gate: bfloat16 [2048, 8192], P('tp', 'ep'), may hold values from -0.125 to 0.125
- dense_up: bfloat16 [2048, 8192], P('tp', 'ep'), may hold values from -0.125 to 0.125
- dense_down: bfloat16 [8192, 2048], P('ep', 'tp'), may hold values from -0.0625 to 0.0625
- route_ids: int32 [1024, 4], P('ep'), may hold values from 0 to 63, all different within a row; in each aligned block of 16 rows (0 to 15, 16 to 31, ...) at most 2 rows name the same one
- route_weights: float32 [1024, 4], P('ep'), may hold values from 0.1 to 1
- expert_gate: bfloat16 [64, 2048, 1024], P('ep', None, 'tp'), may hold values from -0.4375 to 0.4375
- expert_up: bfloat16 [64, 2048, 1024], P('ep', None, 'tp'), may hold values from -0.4375 to 0.4375
- expert_down: bfloat16 [64, 1024, 2048], P('ep', 'tp'), may hold values from -0.01953125 to 0.01953125
Outputs:
- layer_out: bfloat16 [1024, 2048], P('ep', 'tp')
- new_keys: bfloat16 [1024, 512], P('ep', 'tp')
- new_values: bfloat16 [1024, 512], P('ep', 'tp')
Inputs may be any that keep to these rules, and one draw needn't show every extreme that they name: `route_ids`: each row names 4 different experts. Among the rows of one device no expert is named more than 2 times, a bound that some block reaches. Sequence b's cache holds keys at positions below lengths[b]; some sequence fills its whole cache.
All inputs are finite; a program needn't handle non-finite values. No bound on the sum of `lengths` on one device may be relied on, other than what follows from the above.
Results may differ from a plain program's by a relative error of at most 0.011.
Values may be sent and summed in bfloat16 or wider, within the bound.
A program may use at most 64 MiB of HBM per device.

v0:
```python
import jax
import jax.numpy as jnp
from jax import lax
from jax.sharding import Mesh
from jax.sharding import PartitionSpec as P

EP = ("ep_0", "ep_1", "ep_2")


norm_eps = 1e-05
clamp_limit = 7.0
swish_alpha = 1.702


def in_one_piece(arrays, axis, dim, along):
    widths = [a.shape[along] for a in arrays]
    both = jnp.concatenate(arrays, axis=along)
    whole = lax.all_gather(both, axis, axis=dim, tiled=True)
    return tuple(jnp.split(whole, [sum(widths[:k]) for k in range(1, len(widths))], axis=along))


def laid_out(blocks, dim):
    dims = list(blocks.shape[1:])
    dims[dim] *= blocks.shape[0]
    return jnp.moveaxis(blocks, 0, dim).reshape(dims)


def from_everyone(shard, axis):
    count = lax.axis_size(axis)
    return lax.all_to_all(
        jnp.broadcast_to(shard[None], (count, *shard.shape)), axis, 0, 0, tiled=True
    )


def gather_directly(shard, axis, dim):
    return laid_out(from_everyone(shard, axis), dim)


def over_copies(shard, axis):
    everything = from_everyone(shard, axis)
    return jnp.sum(everything, axis=0)


def split_up(shard, dim, count):
    before, after = (shard.shape[:dim], shard.shape[dim + 1 :])
    return jnp.moveaxis(shard.reshape(*before, count, -1, *after), dim, 0)


def summed_on_arrival(shard, axis, dim):
    blocks = split_up(shard, dim, lax.axis_size(axis))
    arrived = lax.all_to_all(blocks, axis, split_axis=0, concat_axis=0, tiled=True)
    return arrived.astype(jnp.float32).sum(axis=0)


def all_blocks(shard, axes, sequence):
    blocks = shard[None]
    for k in sequence:
        blocks = lax.all_gather(blocks, axes[k], axis=0, tiled=True)
    current = [lax.axis_size(axes[k]) for k in reversed(sequence)]
    blocks = blocks.reshape(*current, *shard.shape)
    turned = sorted(range(len(sequence)), key=lambda place: sequence[len(sequence) - 1 - place])
    return blocks.transpose(*turned, *range(len(sequence), blocks.ndim)).reshape(-1, *shard.shape)


def gathered_by_axis(shard, axes, sequence, dim):
    return laid_out(all_blocks(shard, axes, sequence), dim)


def of_everyone(shard, axis):
    return from_everyone(shard, axis).astype(jnp.float32).sum(axis=0)


def rms_scale(values, gain):
    return values * lax.rsqrt(jnp.mean(values * values, axis=-1, keepdims=True) + norm_eps) * gain


def clamped_unit(gate_pre, up_pre):
    gate_c = jnp.minimum(gate_pre, clamp_limit)
    up_c = jnp.clip(up_pre, -clamp_limit, clamp_limit)
    return (up_c + 1.0) * gate_c * jax.nn.sigmoid(swish_alpha * gate_c)


def slot_ranks(flat_ids, expert_count):
    one_hot = (flat_ids[..., None] == jnp.arange(expert_count, dtype=jnp.int32)).astype(jnp.int32)
    earlier = jnp.cumsum(one_hot, axis=-2) - one_hot
    return jnp.sum(earlier * one_hot, axis=-1)


def body(
    tokens,
    attn_gain,
    query_weight,
    key_weight,
    value_weight,
    break_bias,
    cache_keys,
    cache_values,
    lengths,
    out_weight,
    ffn_gain,
    branch_gate,
    dense_gate,
    dense_up,
    dense_down,
    route_ids,
    route_weights,
    expert_gate,
    expert_up,
    expert_down,
):
    ep_count = lax.axis_size(EP)
    tp_count = lax.axis_size("tp")
    seq_count, model_width = tokens.shape
    top_count = route_ids.shape[1]
    local_experts = expert_gate.shape[0]
    expert_count = ep_count * local_experts
    capacity = 2 * seq_count * top_count // expert_count
    slice_width = model_width // tp_count
    tp_start = lax.axis_index("tp") * slice_width
    q_columns = query_weight.shape[1]
    normed = rms_scale(tokens.astype(jnp.float32), attn_gain).astype(jnp.bfloat16)
    pieces = in_one_piece((query_weight, key_weight, value_weight), EP, 0, 1)
    query_sum = jnp.dot(normed, pieces[0], preferred_element_type=jnp.float32)
    key_sum = jnp.dot(normed, pieces[1], preferred_element_type=jnp.float32)
    value_sum = jnp.dot(normed, pieces[2], preferred_element_type=jnp.float32)
    queries = query_sum.astype(jnp.bfloat16)
    new_keys = key_sum.astype(jnp.bfloat16)
    new_values = value_sum.astype(jnp.bfloat16)
    kv_local = cache_keys.shape[1]
    cache_span = cache_keys.shape[2]
    head_dim = cache_keys.shape[3]
    group_size = q_columns // (kv_local * head_dim)
    query_heads = queries.reshape(seq_count, kv_local, group_size, head_dim)
    scores = jnp.einsum(
        "sgrd,sgld->sgrl", query_heads, cache_keys, preferred_element_type=jnp.float32
    )
    scores = (
        scores * head_dim ** (-0.5) + break_bias.reshape(kv_local, group_size)[None, :, :, None]
    )
    positions = lax.broadcasted_iota(jnp.int32, (1, 1, 1, cache_span), 3)
    inside = positions < lengths[:, None, None, None]
    log_keep = jnp.where(inside, jax.nn.log_sigmoid(-scores), 0.0)
    between = lax.cumsum(log_keep, axis=3, reverse=True) - log_keep
    weights = jnp.where(inside, jnp.exp(jax.nn.log_sigmoid(scores) + between), 0.0).astype(
        jnp.bfloat16
    )
    attended = jnp.einsum(
        "sgrl,sgld->sgrd", weights, cache_values, preferred_element_type=jnp.float32
    )
    attended = attended.astype(jnp.bfloat16).reshape(seq_count, q_columns)
    partial_out = jnp.dot(
        attended, gather_directly(out_weight, EP, 1), preferred_element_type=jnp.float32
    )
    mixed_rows = over_copies(partial_out, "tp").astype(jnp.bfloat16)
    resid = tokens.astype(jnp.float32) + mixed_rows.astype(jnp.float32)
    normed2 = rms_scale(resid, ffn_gain).astype(jnp.bfloat16)
    flat_ids = route_ids.reshape(seq_count * top_count)
    slots = (flat_ids * capacity + slot_ranks(flat_ids, expert_count)).reshape(seq_count, top_count)
    dispatch = (
        slots[None, :, :] == jnp.arange(expert_count * capacity, dtype=jnp.int32)[:, None, None]
    )
    dispatch = jnp.any(dispatch, axis=2).astype(jnp.bfloat16)
    outgoing = jnp.dot(dispatch, normed2, preferred_element_type=jnp.float32).astype(jnp.bfloat16)
    outgoing = outgoing.reshape(ep_count, local_experts, capacity, model_width)
    buffer = lax.all_to_all(outgoing, EP, split_axis=0, concat_axis=0, tiled=True)
    gate_pre = jnp.einsum("sxcd,xdw->sxcw", buffer, expert_gate, preferred_element_type=jnp.float32)
    up_pre = jnp.einsum("sxcd,xdw->sxcw", buffer, expert_up, preferred_element_type=jnp.float32)
    activation = clamped_unit(gate_pre, up_pre).astype(jnp.bfloat16)
    partial_rows = jnp.einsum(
        "sxcw,xwd->sxcd", activation, expert_down, preferred_element_type=jnp.float32
    )
    results = summed_on_arrival(partial_rows.astype(jnp.bfloat16), "tp", 3).astype(jnp.bfloat16)
    returned = lax.all_to_all(results, EP, split_axis=0, concat_axis=0, tiled=True)
    returned = returned.reshape(expert_count * capacity, slice_width)
    picked = returned[slots].astype(jnp.float32)
    moe_own = jnp.sum(picked * route_weights[:, :, None], axis=1)
    own_slice = lax.dynamic_slice_in_dim(normed2, tp_start, slice_width, 1)
    piece_rows = gathered_by_axis(own_slice, EP, (1, 0, 2), 0)
    dense_pre = jnp.concatenate(
        [
            jnp.dot(piece_rows, dense_gate, preferred_element_type=jnp.float32),
            jnp.dot(piece_rows, dense_up, preferred_element_type=jnp.float32),
        ],
        axis=1,
    )
    pre_sum = of_everyone(dense_pre.astype(jnp.bfloat16), "tp").astype(jnp.float32)
    dense_cols = dense_gate.shape[1]
    hidden_units = (jax.nn.silu(pre_sum[:, :dense_cols]) * pre_sum[:, dense_cols:]).astype(
        jnp.bfloat16
    )
    dense_block = jnp.dot(hidden_units, dense_down, preferred_element_type=jnp.float32)
    combined = summed_on_arrival(dense_block.astype(jnp.bfloat16), EP, 0)
    resid_own = lax.dynamic_slice_in_dim(resid, tp_start, slice_width, 1)
    branch_own = jax.nn.sigmoid(jnp.dot(normed2, branch_gate, preferred_element_type=jnp.float32))
    layer_sum = resid_own + moe_own + branch_own[:, None] * combined
    return (layer_sum.astype(jnp.bfloat16), new_keys, new_values)


def solution(mesh):
    split = Mesh(mesh.devices.reshape(8, 4, 2, mesh.shape["tp"]), ("ep_0", "ep_1", "ep_2", "tp"))
    return jax.shard_map(
        body,
        mesh=split,
        in_specs=(
            P(EP, None),
            P(),
            P(EP, "tp"),
            P(EP, "tp"),
            P(EP, "tp"),
            P("tp"),
            P(EP, "tp", None, None),
            P(EP, "tp", None, None),
            P(EP),
            P("tp", EP),
            P(),
            P(),
            P("tp", EP),
            P("tp", EP),
            P(EP, "tp"),
            P(EP, None),
            P(EP, None),
            P(EP, None, "tp"),
            P(EP, None, "tp"),
            P(EP, "tp", None),
        ),
        out_specs=(P(EP, "tp"), P(EP, "tp"), P(EP, "tp")),
        check_vma=False,
    )
```

profile of v0, /device:TPU:1, one launch (start us, length us, event | category | flops | bytes accessed | tf_op | source)
XLA Modules:
  0.0 362.7 jit_solution(4714251275176345074)
XLA Ops:
  7.2 1.5 pad_maximum_fusion.1
  8.8 2.4 broadcast_in_dim.25
  11.2 13.1 %all-to-all-start = ((bf16[64,512,32]{1,2,0:T(8,128)(2,1)}), bf16[64,512,32]{1,2,0:T(8,128)(2,1)S(1)}, u32[]{:S(2)}, u32[]{:S(2)}) async-start(bf16[64,512,32]{1,2,0:T(8,128)(2,1)} %broadcast_in_dim.25), calls=%async_computation | async-start | bytes 4194304 | tf_op jit(solution)/shard_map/all_to_all | solution.py:30
  24.9 70.4 %all-gather.4.cloned.1.call-done = bf16[2048,768]{1,0:T(8,128)(2,1)} async-done(((bf16[32,768]{1,0:T(8,128)(2,1)}), bf16[2048,768]{1,0:T(8,128)(2,1)}) %all-gather.4.cloned.1.call-update) | async-done | bytes 3145744 | tf_op jit(solution)/shard_map/all_gather | solution.py:18
  95.3 2.0 fusion.16
  97.4 4.1 %fusion.46 = (f32[16,4,1024]{2,1,0:T(4,128)S(1)}, f32[16,4,1024]{2,1,0:T(4,128)}) fusion(pred[16,1024]{1,0:T(8,128)(4,1)S(1)} %iota_compare_fusion, f32[4]{0:T(128)S(1)} %copy-done.11, bf16[16,4,128]{2,1,0:T(4,128)(2,1)S(1)} %reshape.195, bf16[16,1,1024,128]{3,2,1,0:T(8,128)(2,1)} %param.26), kind=kOutput, calls=%fused_computation.52 | convolution fusion | flops 17432576 | bytes 4751376 | tf_op jit(solution)/shard_map/sgrd,sgld->sgrl/dot_general | solution.py:134
  101.5 0.8 reshape.197
  102.3 79.8 %reduce-window.6 = f32[16,1,4,8,128]{4,3,2,1,0:T(8,128)S(1)} reduce-window(f32[16,1,4,8,128]{4,3,2,1,0:T(8,128)} %bitcast.95, f32[]{:T(128)} %constant.16.clone.1), window={size=1x1x1x1x128 pad=0_0x0_0x0_0x0_0x0_127}, to_apply=%region_1.2 | reduce-window | flops 8323072 | bytes 524292 | tf_op jit(solution)/shard_map/reduce-window
  182.1 0.8 reshape.198
  182.9 0.3 copy.61
  183.4 0.8 reshape.201
  184.2 3.5 fusion.19
  187.7 0.6 fusion.65
  188.4 0.8 broadcast_in_dim.26
  189.2 4.4 %all-to-all-start.1 = ((f32[4,16,2048]{2,1,0:T(8,128)}), f32[4,16,2048]{2,1,0:T(8,128)S(1)}, u32[]{:S(2)}, u32[]{:S(2)}) async-start(f32[4,16,2048]{2,1,0:T(8,128)} %broadcast_in_dim.26), calls=%async_computation.1 | async-start | bytes 1048576 | tf_op jit(solution)/shard_map/all_to_all | solution.py:30
  193.6 0.2 select_reduce_fusion
  194.0 8.6 %all-to-all-done.1 = f32[4,16,2048]{2,1,0:T(8,128)S(1)} async-done(((f32[4,16,2048]{2,1,0:T(8,128)}), f32[4,16,2048]{2,1,0:T(8,128)S(1)}, u32[]{:S(2)}, u32[]{:S(2)}) %all-to-all-start.1) | async-done | bytes 524320 | tf_op jit(solution)/shard_map/all_to_all | solution.py:30
  202.9 0.3 convolution_convert_fusion.1
  203.2 1.2 reshape.205
  204.4 7.8 %all-to-all-start.2 = ((bf16[64,1,2,2048]{3,2,1,0:T(2,128)(2,1)}), bf16[64,1,2,2048]{3,2,1,0:T(2,128)(2,1)S(1)}, u32[]{:S(2)}, u32[]{:S(2)}) async-start(bf16[64,1,2,2048]{3,2,1,0:T(2,128)(2,1)} %bitcast.7), calls=%async_computation.2 | async-start | bytes 1048576 | tf_op jit(solution)/shard_map/all_to_all | solution.py:165
  212.3 10.4 %all-gather = bf16[64,512]{1,0:T(8,128)(2,1)S(1)} all-gather(bf16[16,512]{1,0:T(8,128)(2,1)S(1)} %constant_dynamic-slice_fusion), channel_id=2, replica_groups=mesh['ep_0'=8,'ep_1'=4,'ep_2'=2,'tp'=4] {'ep_1'}, dimensions={0}, use_global_device_ids=true | all-gather | bytes 81920 | tf_op jit(solution)/shard_map/all_gather | solution.py:58
  222.7 22.8 %all_gather.14 = bf16[32,16,512]{2,1,0:T(8,128)(2,1)} all-gather(bf16[4,16,512]{2,1,0:T(8,128)(2,1)S(1)} %bitcast.98), channel_id=1, replica_groups=mesh['ep_0'=8,'ep_1'=4,'ep_2'=2,'tp'=4] {'ep_0'}, dimensions={0}, use_global_device_ids=true | all-gather | bytes 589824 | tf_op jit(solution)/shard_map/all_gather | solution.py:58
  245.5 1.6 convolution_minimum_fusion
  247.1 0.8 convolution_convert_fusion
  247.9 0.9 copy.91
  248.8 3.5 all-to-all-start.3
  252.2 13.7 %all-gather.6.cloned.1.call-done = bf16[64,16,512]{2,1,0:T(8,128)(2,1)} async-done(((bf16[32,16,512]{2,1,0:T(8,128)(2,1)}), bf16[64,16,512]{2,1,0:T(8,128)(2,1)}) %all-gather.6.cloned.1.call-update) | async-done | bytes 1048592 | tf_op jit(solution)/shard_map/all_gather | solution.py:58
  266.0 1.3 copy.72
  267.3 0.5 convolution_convert_fusion.3
  267.8 0.5 convolution_convert_fusion.4
  268.3 0.2 copy.73
  268.6 1.5 broadcast_in_dim.29
  270.1 3.7 %all-to-all-start.5 = ((bf16[4,1024,256]{2,1,0:T(8,128)(2,1)}), bf16[4,1024,256]{2,1,0:T(8,128)(2,1)S(1)}, u32[]{:S(2)}, u32[]{:S(2)}) async-start(bf16[4,1024,256]{2,1,0:T(8,128)(2,1)} %broadcast_in_dim.29), calls=%async_computation.5 | async-start | bytes 4194304 | tf_op jit(solution)/shard_map/all_to_all | solution.py:30
  273.8 1.1 reduce_sum.84
  274.9 0.8 copy.70
  275.7 24.0 %all-to-all-done.5 = bf16[4,1024,256]{2,1,0:T(8,128)(2,1)S(1)} async-done(((bf16[4,1024,256]{2,1,0:T(8,128)(2,1)}), bf16[4,1024,256]{2,1,0:T(8,128)(2,1)S(1)}, u32[]{:S(2)}, u32[]{:S(2)}) %all-to-all-start.5) | async-done | bytes 2097184 | tf_op jit(solution)/shard_map/all_to_all | solution.py:30
  299.7 11.3 %all-to-all-start.4 = ((bf16[64,1,2,512]{3,2,1,0:T(2,128)(2,1)}), bf16[64,1,2,512]{3,2,1,0:T(2,128)(2,1)S(1)}, u32[]{:S(2)}, u32[]{:S(2)}) async-start(bf16[64,1,2,512]{3,2,1,0:T(2,128)(2,1)} %copy.70), calls=%async_computation.4 | async-start | bytes 262144 | tf_op jit(solution)/shard_map/all_to_all | solution.py:173
  311.1 0.3 convert_reduce_fusion
  311.4 2.3 convolution_convert_fusion.2
  313.8 8.4 %all-to-all-done.4 = bf16[64,1,2,512]{3,2,1,0:T(2,128)(2,1)S(1)} async-done(((bf16[64,1,2,512]{3,2,1,0:T(2,128)(2,1)}), bf16[64,1,2,512]{3,2,1,0:T(2,128)(2,1)S(1)}, u32[]{:S(2)}, u32[]{:S(2)}) %all-to-all-start.4) | async-done | bytes 131104 | tf_op jit(solution)/shard_map/all_to_all | solution.py:173
  322.2 4.5 %all-to-all-start.6 = ((bf16[64,16,512]{2,1,0:T(8,128)(2,1)}), bf16[64,16,512]{2,1,0:T(8,128)(2,1)S(1)}, u32[]{:S(2)}, u32[]{:S(2)}) async-start(bf16[64,16,512]{2,1,0:T(8,128)(2,1)} %bitcast.25), calls=%async_computation.6 | async-start | bytes 2097152 | tf_op jit(solution)/shard_map/all_to_all | solution.py:51
  326.9 1.9 convolution_convert_fusion.5
  328.8 1.9 convolution_convert_fusion.6
  330.9 0.7 gather_fusion
  331.6 0.1 multiply_reduce_fusion
  331.8 23.2 %all-to-all-done.6 = bf16[64,16,512]{2,1,0:T(8,128)(2,1)S(1)} async-done(((bf16[64,16,512]{2,1,0:T(8,128)(2,1)}), bf16[64,16,512]{2,1,0:T(8,128)(2,1)S(1)}, u32[]{:S(2)}, u32[]{:S(2)}) %all-to-all-start.6) | async-done | bytes 1048608 | tf_op jit(solution)/shard_map/all_to_all | solution.py:51
  355.0 0.2 convert_reduce_fusion.1
  355.1 0.7 add_convert_fusion
  (70 shorter events, 2.1 us)
Async XLA Ops:
  7.2 239.9 %copy-start = (bf16[1,256,2048]{2,1,0:T(8,128)(2,1)S(1)}, bf16[1,256,2048]{2,1,0:T(8,128)(2,1)}, u32[]{:S(2)}) copy-start(bf16[1,256,2048]{2,1,0:T(8,128)(2,1)} %param.39) | copy-start | bytes 3145732
  7.2 88.2 %all-gather.4.cloned.1.call-start = ((), (), s32[]{:S(2)}) async-start(), calls=%async_computation.7 | async-start | bytes 3194880 | tf_op jit(solution)/shard_map/all_gather | solution.py:18
  8.7 15.6 %copy-start.9 = (s32[16,4]{0,1:T(4,128)S(1)}, s32[16,4]{0,1:T(4,128)}, u32[]{:S(2)}) copy-start(s32[16,4]{0,1:T(4,128)} %param.35) | copy-start | bytes 772
  8.7 15.9 %copy-start.3 = (bf16[16,2048]{1,0:T(8,128)(2,1)S(1)}, bf16[16,2048]{1,0:T(8,128)(2,1)}, u32[]{:S(2)}) copy-start(bf16[16,2048]{1,0:T(8,128)(2,1)} %param.20) | copy-start | bytes 196612
  8.8 16.0 %copy-start.12 = (s32[16]{0:T(128)S(1)}, s32[16]{0:T(128)}, u32[]{:S(2)}) copy-start(s32[16]{0:T(128)} %param.28) | copy-start | bytes 196
  8.8 86.6 %copy-start.13 = (f32[2048]{0:T(1024)S(1)}, f32[2048]{0:T(1024)}, u32[]{:S(2)}) copy-start(f32[2048]{0:T(1024)} %param.21) | copy-start | bytes 24580
  11.2 86.2 %copy-start.11 = (f32[4]{0:T(128)S(1)}, f32[4]{0:T(128)}, u32[]{:S(2)}) copy-start(f32[4]{0:T(128)} %param.25) | copy-start | bytes 52
  11.2 176.5 %all-to-all-start = ((bf16[64,512,32]{1,2,0:T(8,128)(2,1)}), bf16[64,512,32]{1,2,0:T(8,128)(2,1)S(1)}, u32[]{:S(2)}, u32[]{:S(2)}) async-start(bf16[64,512,32]{1,2,0:T(8,128)(2,1)} %broadcast_in_dim.25), calls=%async_computation | async-start | bytes 4194304 | tf_op jit(solution)/shard_map/all_to_all | solution.py:30
  24.8 70.5 %copy-start.15 = (f32[16]{0:T(128)}, f32[16]{0:T(128)S(1)}, u32[]{:S(2)}) copy-start(f32[16]{0:T(128)S(1)} %add_rsqrt_fusion.1) | copy-start | bytes 196
  24.9 76.6 %copy-start.6 = (pred[16,1024]{1,0:T(8,128)(4,1)}, pred[16,1024]{1,0:T(8,128)(4,1)S(1)}, u32[]{:S(2)}) copy-start(pred[16,1024]{1,0:T(8,128)(4,1)S(1)} %iota_compare_fusion) | copy-start | bytes 49156
  187.7 15.1 %copy-start.7 = (f32[2048]{0:T(1024)S(1)}, f32[2048]{0:T(1024)}, u32[]{:S(2)}) copy-start(f32[2048]{0:T(1024)} %param.30) | copy-start | bytes 24580
  189.2 13.4 %all-to-all-start.1 = ((f32[4,16,2048]{2,1,0:T(8,128)}), f32[4,16,2048]{2,1,0:T(8,128)S(1)}, u32[]{:S(2)}, u32[]{:S(2)}) async-start(f32[4,16,2048]{2,1,0:T(8,128)} %broadcast_in_dim.26), calls=%async_computation.1 | async-start | bytes 1048576 | tf_op jit(solution)/shard_map/all_to_all | solution.py:30
  202.6 44.5 %copy-start.2 = (bf16[1,2048,256]{2,1,0:T(8,128)(2,1)S(1)}, bf16[1,2048,256]{2,1,0:T(8,128)(2,1)}, u32[]{:S(2)}) copy-start(bf16[1,2048,256]{2,1,0:T(8,128)(2,1)} %param.38) | copy-start | bytes 3145732
  204.4 41.1 %all-to-all-start.2 = ((bf16[64,1,2,2048]{3,2,1,0:T(2,128)(2,1)}), bf16[64,1,2,2048]{3,2,1,0:T(2,128)(2,1)S(1)}, u32[]{:S(2)}, u32[]{:S(2)}) async-start(bf16[64,1,2,2048]{3,2,1,0:T(2,128)(2,1)} %bitcast.7), calls=%async_computation.2 | async-start | bytes 1048576 | tf_op jit(solution)/shard_map/all_to_all | solution.py:165
  212.2 53.8 %all-gather.6.cloned.1.call-start = ((), (), s32[]{:S(2)}) async-start(), calls=%async_computation.8 | async-start | bytes 1572864 | tf_op jit(solution)/shard_map/all_gather | solution.py:58
  247.9 19.4 %copy-start.4 = (bf16[512,128]{1,0:T(8,128)(2,1)S(1)}, bf16[512,128]{1,0:T(8,128)(2,1)}, u32[]{:S(2)}) copy-start(bf16[512,128]{1,0:T(8,128)(2,1)} %param.33) | copy-start | bytes 393220
  247.9 19.9 %copy-start.5 = (bf16[512,128]{1,0:T(8,128)(2,1)S(1)}, bf16[512,128]{1,0:T(8,128)(2,1)}, u32[]{:S(2)}) copy-start(bf16[512,128]{1,0:T(8,128)(2,1)} %param.32) | copy-start | bytes 393220
  248.8 19.8 %all-to-all-start.3 = ((bf16[4,64,1,2,512]{4,1,3,2,0:T(8,128)(2,1)}), bf16[4,64,1,2,512]{4,1,3,2,0:T(8,128)(2,1)S(1)}, u32[]{:S(2)}, u32[]{:S(2)}) async-start(bf16[4,64,1,2,512]{4,1,3,2,0:T(8,128)(2,1)} %bitcast.88), calls=%async_computation.3 | async-start | bytes 1048576 | tf_op jit(solution)/shard_map/all_to_all | solution.py:51
  268.5 1.5 copy-start.1
  270.1 29.7 %all-to-all-start.5 = ((bf16[4,1024,256]{2,1,0:T(8,128)(2,1)}), bf16[4,1024,256]{2,1,0:T(8,128)(2,1)S(1)}, u32[]{:S(2)}, u32[]{:S(2)}) async-start(bf16[4,1024,256]{2,1,0:T(8,128)(2,1)} %broadcast_in_dim.29), calls=%async_computation.5 | async-start | bytes 4194304 | tf_op jit(solution)/shard_map/all_to_all | solution.py:30
  299.7 22.4 %all-to-all-start.4 = ((bf16[64,1,2,512]{3,2,1,0:T(2,128)(2,1)}), bf16[64,1,2,512]{3,2,1,0:T(2,128)(2,1)S(1)}, u32[]{:S(2)}, u32[]{:S(2)}) async-start(bf16[64,1,2,512]{3,2,1,0:T(2,128)(2,1)} %copy.70), calls=%async_computation.4 | async-start | bytes 262144 | tf_op jit(solution)/shard_map/all_to_all | solution.py:173
  311.4 15.3 %copy-start.8 = (bf16[2048]{0:T(1024)(128)(2,1)S(1)}, bf16[2048]{0:T(1024)(128)(2,1)}, u32[]{:S(2)}) copy-start(bf16[2048]{0:T(1024)(128)(2,1)} %param.31) | copy-start | bytes 12292
  311.4 15.3 %copy-start.10 = (f32[16,4]{0,1:T(4,128)S(1)}, f32[16,4]{0,1:T(4,128)}, u32[]{:S(2)}) copy-start(f32[16,4]{0,1:T(4,128)} %param.36) | copy-start | bytes 772
  311.4 15.5 %copy-start.14 = (f32[2048]{0:T(1024)S(1)}, f32[2048]{0:T(1024)}, u32[]{:S(2)}) copy-start(f32[2048]{0:T(1024)} %param.21) | copy-start | bytes 24580
  311.4 15.5 %copy-start.16 = (f32[16]{0:T(128)S(1)}, f32[16]{0:T(128)}, u32[]{:S(2)}) copy-start(f32[16]{0:T(128)} %copy-done.15) | copy-start | bytes 196
  322.2 32.8 %all-to-all-start.6 = ((bf16[64,16,512]{2,1,0:T(8,128)(2,1)}), bf16[64,16,512]{2,1,0:T(8,128)(2,1)S(1)}, u32[]{:S(2)}, u32[]{:S(2)}) async-start(bf16[64,16,512]{2,1,0:T(8,128)(2,1)} %bitcast.25), calls=%async_computation.6 | async-start | bytes 2097152 | tf_op jit(solution)/shard_map/all_to_all | solution.py:51
Sparse Core Ops, SparseCore 0:
  10.7 84.5 all-gather.3
  245.6 20.3 all-gather.5
where the time goes:
time: 364 us; the launch traced here: 363 us
  waiting for transfers between devices  148 us (41%)
  other arithmetic  84.7 us (23%)
  starting transfers between devices  48.4 us (13%)
  blocking collectives  33.2 us (9%)
  matrix products  20.1 us (6%)
  between operations  14.5 us (4%)
  local copies, waits for them, and re-layouts  13.4 us (4%)
    another operation x2, other arithmetic  79.8 us
    all_gather x1, waiting for transfers between devices, in_one_piece(): whole = lax.all_gather(both, axis, axis=dim, tiled=True)  70.4 us
    all_gather x2, blocking collectives, all_blocks(): blocks = lax.all_gather(blocks, axes[k], axis=0, tiled=True)  33.2 us
    all_to_all x3, waiting for transfers between devices, from_everyone(): lax.all_to_all(jnp.broadcast_to(shard[None], (count, *shard.shape)), axis...  32.6 us
    all_to_all x2, waiting for transfers between devices, summed_on_arrival(): lax.all_to_all(blocks, axis, split_axis=0, concat_axis=0, tiled=True)  23.2 us
    all_to_all x3, starting transfers between devices, from_everyone(): lax.all_to_all(jnp.broadcast_to(shard[None], (count, *shard.shape)), axis...  21.2 us
    all_gather x1, waiting for transfers between devices, all_blocks(): blocks = lax.all_gather(blocks, axes[k], axis=0, tiled=True)  13.7 us
    all_to_all x1, starting transfers between devices, body(): lax.all_to_all(results, EP, split_axis=0, concat_axis=0, tiled=True)  11.3 us
  transfers between devices with their start and end apart: 9, of which 6 were waited for; matrix products, arithmetic and copies ran while one was open for 31% of the time, Pallas kernels for 0%

commit v1 on v0

v1 whole, which is shorter than its diff:
```python
import functools

import jax
import jax.numpy as jnp
from jax import lax
from jax.experimental import pallas as pl
from jax.experimental.pallas import tpu as pltpu
from jax.sharding import Mesh
from jax.sharding import PartitionSpec as P

EP = ("z", "x", "c")
NZ, NX, NC, NT = 8, 4, 2, 4
NJ = NX * NC

norm_eps = 1e-05
clamp_limit = 7.0
swish_alpha = 1.702

BF = jnp.bfloat16
F32 = jnp.float32
MESH_IDS = pl.DeviceIdType.MESH


def dot(a, b):
    return jnp.dot(a, b, preferred_element_type=F32)


def dot_nt(a, b):
    return lax.dot_general(a, b, (((1,), (1,)), ((), ())), preferred_element_type=F32)


def iota(shape, dim):
    return lax.broadcasted_iota(jnp.int32, shape, dim)


def one_if(mask):
    return jnp.where(mask, 1.0, 0.0)


def kernel(
    tokens,
    attn_gain,
    wq_in,
    wk_in,
    wv_in,
    bias,
    keys_hbm,
    values_hbm,
    lengths,
    wo_in,
    ffn_gain,
    branch_gate,
    dgate_hbm,
    dup_hbm,
    ddown_hbm,
    route_ids,
    route_weights,
    egate_hbm,
    eup_hbm,
    edown_hbm,
    layer_out,
    new_keys,
    new_values,
    keys,
    values,
    egate,
    eup,
    edown,
    dgate,
    dup,
    ddown,
    wq,
    wk,
    wv,
    wo,
    nsend,
    nslab,
    qsend,
    qrecv,
    scores,
    q64,
    att64,
    att_all,
    wd_all,
    po,
    mx_send,
    mx_recv,
    resid,
    xs,
    row_send,
    row_recv,
    pd_send,
    pd_recv,
    hid,
    pe_send,
    pe_recv,
    er,
    er_recv,
    dense_part,
    fin_send,
    fin_recv,
    local_sem,
    kv_sem,
    z_send,
    z_recv,
    j_send,
    j_recv,
    t_send,
    t_recv,
):
    mz = lax.axis_index("z")
    mxx = lax.axis_index("x")
    mc = lax.axis_index("c")
    mt = lax.axis_index("tp")
    mj = mxx * NC + mc

    def zpeer(d):
        return lax.rem(mz + d, NZ)

    def jpeer(d):
        return lax.rem(mj + d, NJ)

    def tpeer(d):
        return lax.rem(mt + d, NT)

    def zdev(d):
        return {"z": zpeer(d)}

    def jdev(d):
        j = jpeer(d)
        return {"x": lax.div(j, NC), "c": lax.rem(j, NC)}

    def tdev(d):
        return {"tp": tpeer(d)}

    def remote(src, dst, ssem, rsem, dev):
        return pltpu.make_async_remote_copy(
            src_ref=src,
            dst_ref=dst,
            send_sem=ssem,
            recv_sem=rsem,
            device_id=dev,
            device_id_type=MESH_IDS,
        )

    started = []

    def exchange(n, make):
        copies = [make(d) for d in range(1, n)]
        for copy in copies:
            copy.start()
        started.extend(copies)
        return copies

    def arrived(copies):
        for copy in copies:
            copy.wait_recv()

    locals_ = []
    kv_copies = []
    for s in range(0, 16, 2):
        kv_copies.append(
            pltpu.make_async_copy(
                keys_hbm.at[pl.ds(s, 2), 0], keys.at[pl.ds(s, 2)], kv_sem.at[s]
            )
        )
        kv_copies.append(
            pltpu.make_async_copy(
                values_hbm.at[pl.ds(s, 2), 0], values.at[pl.ds(s, 2)], kv_sem.at[s + 1]
            )
        )
    for copy in kv_copies:
        copy.start()
    dense_col = pl.ds(pl.multiple_of(mj * 128, 128), 128)
    locals_.append(pltpu.make_async_copy(dgate_hbm, dgate.at[:, dense_col], local_sem.at[0]))
    locals_.append(pltpu.make_async_copy(dup_hbm, dup.at[:, dense_col], local_sem.at[1]))
    locals_.append(pltpu.make_async_copy(ddown_hbm, ddown.at[dense_col], local_sem.at[2]))
    locals_.append(pltpu.make_async_copy(egate_hbm.at[0], egate, local_sem.at[3]))
    locals_.append(pltpu.make_async_copy(eup_hbm.at[0], eup, local_sem.at[4]))
    locals_.append(pltpu.make_async_copy(edown_hbm.at[0], edown, local_sem.at[5]))
    for copy in locals_:
        copy.start()

    barrier = pltpu.get_barrier_semaphore()
    for d in range(1, NJ):
        pl.semaphore_signal(barrier, inc=1, device_id=jdev(d), device_id_type=MESH_IDS)
    for d in range(1, NZ):
        pl.semaphore_signal(barrier, inc=1, device_id=zdev(d), device_id_type=MESH_IDS)
    for d in range(1, NT):
        pl.semaphore_signal(barrier, inc=1, device_id=tdev(d), device_id_type=MESH_IDS)

    tok = tokens[...].astype(F32)
    normed = (
        tok * lax.rsqrt(jnp.mean(tok * tok, axis=-1, keepdims=True) + norm_eps) * attn_gain[...]
    ).astype(BF)
    for z in range(NZ):
        nsend[z] = normed[:, 256 * z : 256 * (z + 1)]

    ids = route_ids[...]
    rws = route_weights[...]
    lane_expert = lax.shift_right_logical(iota((16, 128), 1), 1)
    named = jnp.zeros((16, 128), F32)
    weighed = jnp.zeros((16, 128), F32)
    for k in range(4):
        hit = ids[:, k : k + 1] == lane_expert
        named = named + one_if(hit)
        weighed = weighed + jnp.where(hit, rws[:, k : k + 1], 0.0)
    earlier = one_if(iota((16, 16), 1) < iota((16, 16), 0)).astype(BF)
    rank = dot(earlier, named.astype(BF))
    lane_rank = jnp.bitwise_and(iota((16, 128), 1), 1).astype(F32)
    wd_all[mz] = jnp.where(rank == lane_rank, weighed, 0.0)

    pl.semaphore_wait(barrier, NJ + NZ + NT - 3)

    c_wq = exchange(
        NJ, lambda d: remote(wq_in, wq.at[mj], j_send.at[0, d], j_recv.at[0, d], jdev(d))
    )
    c_wk = exchange(
        NJ, lambda d: remote(wk_in, wk.at[mj], j_send.at[1, d], j_recv.at[1, d], jdev(d))
    )
    c_wv = exchange(
        NJ, lambda d: remote(wv_in, wv.at[mj], j_send.at[2, d], j_recv.at[2, d], jdev(d))
    )
    c_n = exchange(
        NZ,
        lambda d: remote(
            nsend.at[zpeer(d)], nslab.at[mz], z_send.at[0, d], z_recv.at[0, d], zdev(d)
        ),
    )
    c_wd = exchange(
        NZ,
        lambda d: remote(
            wd_all.at[mz], wd_all.at[mz], z_send.at[1, d], z_recv.at[1, d], zdev(d)
        ),
    )
    c_wo = exchange(
        NJ, lambda d: remote(wo_in, wo.at[mj], j_send.at[3, d], j_recv.at[3, d], jdev(d))
    )
    c_dg = exchange(
        NJ,
        lambda d: remote(
            dgate_hbm, dgate.at[:, dense_col], j_send.at[4, d], j_recv.at[4, d], jdev(d)
        ),
    )
    c_du = exchange(
        NJ,
        lambda d: remote(
            dup_hbm, dup.at[:, dense_col], j_send.at[5, d], j_recv.at[5, d], jdev(d)
        ),
    )
    c_dd = exchange(
        NJ,
        lambda d: remote(
            ddown_hbm, ddown.at[dense_col], j_send.at[6, d], j_recv.at[6, d], jdev(d)
        ),
    )
    wq[mj] = wq_in[...]
    wk[mj] = wk_in[...]
    wv[mj] = wv_in[...]
    wo[mj] = wo_in[...]
    nslab[mz] = nsend[mz]

    arrived(c_n)
    arrived(c_wq)
    arrived(c_wk)
    arrived(c_wv)
    slab = nslab[...].reshape(128, 256)
    qsend[:, :, 0:512] = dot(slab, wq[...].reshape(256, 512)).astype(BF).reshape(NZ, 16, 512)
    qsend[:, :, 512:640] = dot(slab, wk[...].reshape(256, 128)).astype(BF).reshape(NZ, 16, 128)
    qsend[:, :, 640:768] = dot(slab, wv[...].reshape(256, 128)).astype(BF).reshape(NZ, 16, 128)
    c_q = exchange(
        NZ,
        lambda d: remote(
            qsend.at[zpeer(d)], qrecv.at[mz], z_send.at[2, d], z_recv.at[2, d], zdev(d)
        ),
    )
    qrecv[mz] = qsend[mz]
    arrived(c_q)
    total = qrecv[0].astype(F32)
    for z in range(1, NZ):
        total = total + qrecv[z].astype(F32)
    total = total.astype(BF)
    new_keys[...] = total[:, 512:640]
    new_values[...] = total[:, 640:768]

    q_rows = jnp.zeros((64, 128), F32)
    for h in range(4):
        spread = one_if(iota((64, 16), 0) == 4 * iota((64, 16), 1) + h).astype(BF)
        q_rows = q_rows + dot(spread, total[:, 128 * h : 128 * (h + 1)])
    q64[...] = q_rows
    for copy in kv_copies:
        copy.wait()
    first = iota((8, 128), 0) < 4
    for p in range(8):
        q8 = q64[8 * p : 8 * p + 8]
        qa = jnp.where(first, q8, 0.0).astype(BF)
        qb = jnp.where(first, 0.0, q8).astype(BF)
        scores[8 * p : 8 * p + 8] = dot_nt(qa, keys[2 * p]) + dot_nt(qb, keys[2 * p + 1])

    row = iota((64, 1), 0)
    head = jnp.bitwise_and(row, 3)
    seq = lax.shift_right_logical(row, 2)
    bias_col = jnp.zeros((64, 1), F32)
    for h in range(4):
        bias_col = jnp.where(head == h, bias[h], bias_col)
    len_col = jnp.zeros((64, 1), jnp.int32)
    for s in range(16):
        len_col = jnp.where(seq == s, lengths[s], len_col)
    after = one_if(iota((128, 128), 0) > iota((128, 128), 1)).astype(BF)
    carry = jnp.zeros((64, 1), F32)
    for b in reversed(range(8)):
        cols = slice(128 * b, 128 * (b + 1))
        zz = scores[:, cols] * (128 ** (-0.5)) + bias_col
        inside = (iota((64, 128), 1) + 128 * b) < len_col
        soft = jnp.log1p(jnp.exp(-jnp.abs(zz)))
        keep = jnp.where(inside, jnp.minimum(-zz, 0.0) - soft, 0.0)
        take = jnp.minimum(zz, 0.0) - soft
        k1 = keep.astype(BF)
        r1 = keep - k1.astype(F32)
        k2 = r1.astype(BF)
        k3 = (r1 - k2.astype(F32)).astype(BF)
        between = dot(k1, after) + dot(k2, after) + dot(k3, after) + carry
        carry = between[:, 0:1] + keep[:, 0:1]
        scores[:, cols] = jnp.where(inside, jnp.exp(take + between), 0.0)

    for p in range(8):
        w8 = scores[8 * p : 8 * p + 8].astype(BF)
        att64[8 * p : 8 * p + 8] = jnp.where(
            first, dot(w8, values[2 * p]), dot(w8, values[2 * p + 1])
        )
    att_rows = att64[...].astype(BF)
    for h in range(4):
        pick = one_if(iota((16, 64), 1) == 4 * iota((16, 64), 0) + h).astype(BF)
        att_all[mz, :, 128 * h : 128 * (h + 1)] = dot(pick, att_rows).astype(BF)

    c_a = exchange(
        NZ,
        lambda d: remote(
            att_all.at[mz], att_all.at[mz], z_send.at[3, d], z_recv.at[3, d], zdev(d)
        ),
    )
    arrived(c_wo)
    arrived(c_a)
    po[mt] = dot_nt(att_all[...].reshape(128, 512), wo[...].reshape(256, 512)).astype(BF)
    c_po = exchange(
        NT, lambda d: remote(po.at[mt], po.at[mt], t_send.at[0, d], t_recv.at[0, d], tdev(d))
    )
    arrived(c_po)
    mixed = po[0].astype(F32)
    for t in range(1, NT):
        mixed = mixed + po[t].astype(F32)
    mx_send[...] = mixed.astype(BF).reshape(NZ, 16, 256)
    c_mx = exchange(
        NZ,
        lambda d: remote(
            mx_send.at[zpeer(d)], mx_recv.at[mz], z_send.at[4, d], z_recv.at[4, d], zdev(d)
        ),
    )
    mx_recv[mz] = mx_send[mz]
    arrived(c_mx)
    for z in range(NZ):
        cols = slice(256 * z, 256 * (z + 1))
        resid[:, cols] = tokens[:, cols].astype(F32) + mx_recv[z].astype(F32)
    res = resid[...]
    xs[mz] = (
        res * lax.rsqrt(jnp.mean(res * res, axis=-1, keepdims=True) + norm_eps) * ffn_gain[...]
    ).astype(BF)

    c_x = exchange(
        NZ, lambda d: remote(xs.at[mz], xs.at[mz], z_send.at[5, d], z_recv.at[5, d], zdev(d))
    )
    arrived(c_wd)
    slot_of_row = 16 * mz + 2 * lax.shift_right_logical(iota((128, 128), 0), 4)
    slot_of_row = slot_of_row + jnp.bitwise_and(iota((128, 128), 0), 1)
    spread = one_if(slot_of_row == iota((128, 128), 1)).astype(BF)
    row_z = jnp.bitwise_and(lax.shift_right_logical(iota((128, 128), 0), 1), 7)
    own_z = row_z == lax.shift_right_logical(iota((128, 128), 1), 4)
    wd = wd_all[...].reshape(128, 128)
    wd_hi = wd.astype(BF)
    wd_lo = (wd - wd_hi.astype(F32)).astype(BF)
    filled = one_if(wd > 0.0).astype(BF)
    dispatch = jnp.where(own_z, dot_nt(spread, filled), 0.0).astype(BF)
    row_z_t = jnp.bitwise_and(lax.shift_right_logical(iota((128, 128), 1), 1), 7)
    own_z_t = row_z_t == lax.shift_right_logical(iota((128, 128), 0), 4)
    comb_hi = jnp.where(own_z_t, dot_nt(wd_hi, spread), 0.0).astype(BF)
    comb_lo = jnp.where(own_z_t, dot_nt(wd_lo, spread), 0.0).astype(BF)

    arrived(c_x)
    for b in range(4):
        cols = slice(512 * b, 512 * (b + 1))
        row_send[:, :, cols] = (
            dot(dispatch, xs[:, :, cols].reshape(128, 512)).astype(BF).reshape(NJ, 16, 512)
        )
    c_row = exchange(
        NJ,
        lambda d: remote(
            row_send.at[jpeer(d)], row_recv.at[mj], j_send.at[7, d], j_recv.at[7, d], jdev(d)
        ),
    )
    row_recv[mj] = row_send[mj]

    for copy in locals_:
        copy.wait()
    arrived(c_dg)
    arrived(c_du)
    own_cols = pl.ds(pl.multiple_of(mt * 512, 512), 512)
    x_own = xs[:, :, own_cols].reshape(128, 512)
    for t in range(NT):
        cols = slice(256 * t, 256 * (t + 1))
        pd_send[t, :, 0:256] = dot(x_own, dgate[:, cols]).astype(BF)
        pd_send[t, :, 256:512] = dot(x_own, dup[:, cols]).astype(BF)
    c_pd = exchange(
        NT,
        lambda d: remote(
            pd_send.at[tpeer(d)], pd_recv.at[mt], t_send.at[1, d], t_recv.at[1, d], tdev(d)
        ),
    )
    pd_recv[mt] = pd_send[mt]
    x_all = xs[...].reshape(128, 2048).astype(F32)
    branch = jax.nn.sigmoid(jnp.sum(x_all * branch_gate[...], axis=-1, keepdims=True))
    arrived(c_pd)
    pre = pd_recv[0].astype(F32)
    for t in range(1, NT):
        pre = pre + pd_recv[t].astype(F32)
    gate_d = pre[:, 0:256]
    hid[mt] = (gate_d * jax.nn.sigmoid(gate_d) * pre[:, 256:512]).astype(BF)
    c_h = exchange(
        NT, lambda d: remote(hid.at[mt], hid.at[mt], t_send.at[2, d], t_recv.at[2, d], tdev(d))
    )

    arrived(c_row)
    rows = row_recv[...].reshape(128, 2048)
    gate_c = jnp.minimum(dot(rows, egate[...]), clamp_limit)
    up_c = jnp.clip(dot(rows, eup[...]), -clamp_limit, clamp_limit)
    unit = ((up_c + 1.0) * gate_c * jax.nn.sigmoid(swish_alpha * gate_c)).astype(BF)
    for t in range(NT):
        pe_send[t] = dot(unit, edown[:, 512 * t : 512 * (t + 1)]).astype(BF)
    c_pe = exchange(
        NT,
        lambda d: remote(
            pe_send.at[tpeer(d)], pe_recv.at[mt], t_send.at[3, d], t_recv.at[3, d], tdev(d)
        ),
    )
    pe_recv[mt] = pe_send[mt]

    arrived(c_h)
    arrived(c_dd)
    down = dot(hid[0], ddown[0:256])
    for t in range(1, NT):
        down = down + dot(hid[t], ddown[256 * t : 256 * (t + 1)])
    dense_part[...] = down * branch

    arrived(c_pe)
    total_e = pe_recv[0].astype(F32)
    for t in range(1, NT):
        total_e = total_e + pe_recv[t].astype(F32)
    er[...] = total_e.astype(BF).reshape(NJ, 16, 512)
    c_er = exchange(
        NJ,
        lambda d: remote(
            er.at[jpeer(d)], er_recv.at[mj], j_send.at[8, d], j_recv.at[8, d], jdev(d)
        ),
    )
    er_recv[mj] = er[mj]
    arrived(c_er)
    back = er_recv[...].reshape(128, 512)
    fin_send[...] = (
        (dot(comb_hi, back) + dot(comb_lo, back) + dense_part[...]).astype(BF).reshape(NZ, 16, 512)
    )
    c_f = exchange(
        NZ,
        lambda d: remote(
            fin_send.at[zpeer(d)], fin_recv.at[mz], z_send.at[6, d], z_recv.at[6, d], zdev(d)
        ),
    )
    fin_recv[mz] = fin_send[mz]
    arrived(c_f)
    final = resid[:, own_cols]
    for z in range(NZ):
        final = final + fin_recv[z].astype(F32)
    layer_out[...] = final.astype(BF)

    for copy in started:
        copy.wait_send()


def body(
    tokens,
    attn_gain,
    query_weight,
    key_weight,
    value_weight,
    break_bias,
    cache_keys,
    cache_values,
    lengths,
    out_weight,
    ffn_gain,
    branch_gate,
    dense_gate,
    dense_up,
    dense_down,
    route_ids,
    route_weights,
    expert_gate,
    expert_up,
    expert_down,
):
    vm = pl.BlockSpec(memory_space=pltpu.VMEM)
    sm = pl.BlockSpec(memory_space=pltpu.SMEM)
    hbm = pl.BlockSpec(memory_space=pl.ANY)
    V = pltpu.VMEM
    return tuple(
        pl.pallas_call(
            kernel,
            name="layer",
            out_shape=(
                jax.ShapeDtypeStruct((16, 512), BF),
                jax.ShapeDtypeStruct((16, 128), BF),
                jax.ShapeDtypeStruct((16, 128), BF),
            ),
            in_specs=[
                vm,
                vm,
                vm,
                vm,
                vm,
                sm,
                hbm,
                hbm,
                sm,
                vm,
                vm,
                vm,
                hbm,
                hbm,
                hbm,
                vm,
                vm,
                hbm,
                hbm,
                hbm,
            ],
            out_specs=(vm, vm, vm),
            scratch_shapes=[
                V((16, 1024, 128), BF),
                V((16, 1024, 128), BF),
                V((2048, 256), BF),
                V((2048, 256), BF),
                V((256, 2048), BF),
                V((512, 1024), BF),
                V((512, 1024), BF),
                V((1024, 512), BF),
                V((NJ, 32, 512), BF),
                V((NJ, 32, 128), BF),
                V((NJ, 32, 128), BF),
                V((NJ, 32, 512), BF),
                V((NZ, 16, 256), BF),
                V((NZ, 16, 256), BF),
                V((NZ, 16, 768), BF),
                V((NZ, 16, 768), BF),
                V((64, 1024), F32),
                V((64, 128), F32),
                V((64, 128), F32),
                V((NZ, 16, 512), BF),
                V((NZ, 16, 128), F32),
                V((NT, 128, 256), BF),
                V((NZ, 16, 256), BF),
                V((NZ, 16, 256), BF),
                V((16, 2048), F32),
                V((NZ, 16, 2048), BF),
                V((NJ, 16, 2048), BF),
                V((NJ, 16, 2048), BF),
                V((NT, 128, 512), BF),
                V((NT, 128, 512), BF),
                V((NT, 128, 256), BF),
                V((NT, 128, 512), BF),
                V((NT, 128, 512), BF),
                V((NJ, 16, 512), BF),
                V((NJ, 16, 512), BF),
                V((128, 512), F32),
                V((NZ, 16, 512), BF),
                V((NZ, 16, 512), BF),
                pltpu.SemaphoreType.DMA((6,)),
                pltpu.SemaphoreType.DMA((16,)),
                pltpu.SemaphoreType.DMA((7, NZ)),
                pltpu.SemaphoreType.DMA((7, NZ)),
                pltpu.SemaphoreType.DMA((9, NJ)),
                pltpu.SemaphoreType.DMA((9, NJ)),
                pltpu.SemaphoreType.DMA((4, NT)),
                pltpu.SemaphoreType.DMA((4, NT)),
            ],
            compiler_params=pltpu.CompilerParams(
                collective_id=0,
                has_side_effects=True,
                vmem_limit_bytes=60 * 1024 * 1024,
            ),
        )(
            tokens,
            attn_gain.reshape(1, -1),
            query_weight,
            key_weight,
            value_weight,
            break_bias,
            cache_keys,
            cache_values,
            lengths,
            out_weight.T,
            ffn_gain.reshape(1, -1),
            branch_gate.astype(F32).reshape(1, -1),
            dense_gate,
            dense_up,
            dense_down,
            route_ids,
            route_weights,
            expert_gate,
            expert_up,
            expert_down,
        )
    )


def solution(mesh):
    split = Mesh(mesh.devices.reshape(NZ, NX, NC, NT), ("z", "x", "c", "tp"))
    return jax.shard_map(
        body,
        mesh=split,
        in_specs=(
            P(EP, None),
            P(),
            P(EP, "tp"),
            P(EP, "tp"),
            P(EP, "tp"),
            P("tp"),
            P(EP, "tp", None, None),
            P(EP, "tp", None, None),
            P(EP),
            P("tp", EP),
            P(),
            P(),
            P("tp", EP),
            P("tp", EP),
            P(EP, "tp"),
            P(EP, None),
            P(EP, None),
            P(EP, None, "tp"),
            P(EP, None, "tp"),
            P(EP, "tp", None),
        ),
        out_specs=(P(EP, "tp"), P(EP, "tp"), P(EP, "tp")),
        check_vma=False,
    )
```

time: 364 us -> 96.7 us (0.27)
  waiting for transfers between devices: 148 us -> 0 us
  Pallas kernels: 0 us -> 87.8 us
  other arithmetic: 84.7 us -> 1.29 us
  starting transfers between devices: 48.4 us -> 0 us
  blocking collectives: 33.2 us -> 0 us
  matrix products: 20.1 us -> 0 us
  between operations: 14.5 us -> 0.64 us
  local copies, waits for them, and re-layouts: 13.4 us -> 6.56 us
    pallas_call x0 -> x1, Pallas kernels: none -> 87.8 us  [body(): pl.pallas_call(kernel, name='layer', out_shape=(jax.ShapeDtypeStruct((16,...]
    all_gather x2 -> x0, waiting for transfers between devices: 84.2 us -> none  [the longest x1 70.4 us: in_one_piece(): whole = lax.all_gather(both, axis, axis=dim, tiled=True)]
    another operation x3 -> x0, other arithmetic: 79.9 us -> none
    all_to_all x7 -> x0, waiting for transfers between devices: 64.2 us -> none  [the longest x3 32.6 us: from_everyone(): lax.all_to_all(jnp.broadcast_to(shard[None], (count, *shard.shape)), axis...]
    all_to_all x7 -> x0, starting transfers between devices: 48.3 us -> none  [the longest x3 21.2 us: from_everyone(): lax.all_to_all(jnp.broadcast_to(shard[None], (count, *shard.shape)), axis...]
    all_gather x2 -> x0, blocking collectives: 33.2 us -> none  [all_blocks(): blocks = lax.all_gather(blocks, axes[k], axis=0, tiled=True)]
    dot_general x13 -> x0, matrix products: 20.1 us -> none  [the longest x1 4.08 us: body(): jnp.einsum('sgrd,sgld->sgrl', query_heads, cache_keys, preferred_element_...]
    unnamed x37 -> x5, local copies, waits for them, and re-layouts: 0.28 us -> 6.56 us
  transfers between devices with their start and end apart: 9 -> 0, of which waited for: 6 -> 0; matrix products, arithmetic and copies ran while one was open for 31% -> 0% of each run, Pallas kernels for 0% -> 0%
where the time goes in v1:
time: 96.7 us; the launch traced here: 96.3 us
  Pallas kernels  87.8 us (91%)
  local copies, waits for them, and re-layouts  6.56 us (7%)
  other arithmetic  1.29 us (1%)
    pallas_call x1, Pallas kernels, body(): pl.pallas_call(kernel, name='layer', out_shape=(jax.ShapeDtypeStruct((16,...  87.8 us
    unnamed x5, local copies, waits for them, and re-layouts  6.56 us

profile of v1, /device:TPU:1, one launch (start us, length us, event | category | flops | bytes accessed | tf_op | source)
XLA Modules:
  0.0 96.3 jit_solution(11668728899886667101)
XLA Ops:
  0.6 1.3 %reshape.21 = f32[2048]{0:T(1024)} convert(bf16[2048]{0:T(1024)(128)(2,1)} %param.31) | non-fusion elementwise | flops 2048 | bytes 12288 | tf_op jit(solution)/shard_map/reshape | solution.py:610
  1.9 1.3 %copy.23.route_ids = s32[16,4]{1,0:T(8,128)} copy(s32[16,4]{0,1:T(4,128)} %param.35) | data formatting | bytes 512 | tf_op args[15]
  3.3 1.4 %copy.24.route_weights = f32[16,4]{1,0:T(8,128)} copy(f32[16,4]{0,1:T(4,128)} %param.36) | data formatting | bytes 512 | tf_op args[16]
  4.6 87.8 %layer.1 = (bf16[16,512]{1,0:T(8,128)(2,1)}, bf16[16,128]{1,0:T(8,128)(2,1)}, bf16[16,128]{1,0:T(8,128)(2,1)}) custom-call(bf16[16,2048]{1,0:T(8,128)(2,1)} %tokens.1, f32[1,2048]{1,0:T(1,128)} %bitcast.6, bf16[32,512]{1,0:T(8,128)(2,1)} %wq_in.1, bf16[32,128]{1,0:T(8,128)(2,1)} %wk_in.1, bf16[32,128]{1,0:T(8,128)(2,1)} %wv_in.1, f32[4]{0:T(128)} %bias.1, ...), custom_call_target="tpu_custom_call" | custom-call | tf_op jit(solution)/shard_map/layer/pallas_call | solution.py:514
  92.4 1.3 %copy.28 = bf16[16,512]{1,0:T(8,128)(2,1)} copy(bf16[16,512]{1,0:T(8,128)(2,1)} %get-tuple-element.6) | data formatting | bytes 32768
  93.8 1.3 %copy.29 = bf16[16,128]{1,0:T(8,128)(2,1)} copy(bf16[16,128]{1,0:T(8,128)(2,1)} %get-tuple-element.7) | data formatting | bytes 8192
  95.0 1.3 %copy.30 = bf16[16,128]{1,0:T(8,128)(2,1)} copy(bf16[16,128]{1,0:T(8,128)(2,1)} %get-tuple-element.8) | data formatting | bytes 8192

commit v2 on v1

v2 whole, which is shorter than its diff:
```python
import functools

import jax
import jax.numpy as jnp
from jax import lax
from jax.experimental import pallas as pl
from jax.experimental.pallas import tpu as pltpu
from jax.sharding import Mesh
from jax.sharding import PartitionSpec as P

EP = ("z", "x", "c")
NZ, NX, NC, NT = 8, 4, 2, 4
NJ = NX * NC

norm_eps = 1e-05
clamp_limit = 7.0
swish_alpha = 1.702

BF = jnp.bfloat16
F32 = jnp.float32
MESH_IDS = pl.DeviceIdType.MESH


def dot(a, b):
    return jnp.dot(a, b, preferred_element_type=F32)


def dot_nt(a, b):
    return lax.dot_general(a, b, (((1,), (1,)), ((), ())), preferred_element_type=F32)


def iota(shape, dim):
    return lax.broadcasted_iota(jnp.int32, shape, dim)


def one_if(mask):
    return jnp.where(mask, 1.0, 0.0)


Z_ORDER = (4, 3, 5, 2, 6, 1, 7)
J_ORDER = (4, 3, 5, 2, 6, 1, 7)
T_ORDER = (2, 1, 3)


def kernel(
    tokens_in,
    attn_gain_in,
    wq_hbm,
    wk_hbm,
    wv_hbm,
    bias,
    keys_hbm,
    values_hbm,
    lengths,
    wo_hbm,
    ffn_gain_in,
    branch_gate_in,
    dgate_hbm,
    dup_hbm,
    ddown_hbm,
    route_ids_in,
    route_weights_in,
    egate_hbm,
    eup_hbm,
    edown_hbm,
    out,
    tokens,
    attn_gain,
    wq_in,
    wk_in,
    wv_in,
    wo_in,
    ffn_gain,
    branch_gate,
    route_ids,
    route_weights,
    keys,
    values,
    egate,
    eup,
    edown,
    dgate,
    dup,
    ddown,
    wq,
    wk,
    wv,
    wo,
    nsend,
    nslab,
    qsend,
    qrecv,
    scores,
    q64,
    att64,
    att_all,
    wd_all,
    tok_all,
    po_send,
    po_recv,
    mixed,
    xs,
    row_send,
    row_recv,
    pd_send,
    pd_recv,
    hid,
    pe_send,
    pe_recv,
    er,
    er_recv,
    dense_part,
    fin_send,
    fin_recv,
    in_sem,
    local_sem,
    kv_sem,
    z_send,
    z_recv,
    j_send,
    j_recv,
    t_send,
    t_recv,
    ft_send,
    ft_recv,
    fm_send,
    fm_recv,
):
    mz = lax.axis_index("z")
    mxx = lax.axis_index("x")
    mc = lax.axis_index("c")
    mt = lax.axis_index("tp")
    mj = mxx * NC + mc

    def zpeer(d):
        return lax.rem(mz + d, NZ)

    def zsource(d):
        return lax.rem(mz + NZ - d, NZ)

    def jpeer(d):
        return lax.rem(mj + d, NJ)

    def tpeer(d):
        return lax.rem(mt + d, NT)

    def zdev(d):
        return {"z": zpeer(d)}

    def jdev(d):
        j = jpeer(d)
        return {"x": lax.div(j, NC), "c": lax.rem(j, NC)}

    def tdev(d):
        return {"tp": tpeer(d)}

    def remote(src, dst, ssem, rsem, dev):
        return pltpu.make_async_remote_copy(
            src_ref=src,
            dst_ref=dst,
            send_sem=ssem,
            recv_sem=rsem,
            device_id=dev,
            device_id_type=MESH_IDS,
        )

    started = []

    def exchange(order, make):
        copies = [make(d) for d in order]
        for copy in copies:
            copy.start()
        started.extend(copies)
        return copies

    def arrived(copies):
        for copy in reversed(copies):
            copy.wait_recv()

    barrier = pltpu.get_barrier_semaphore()
    for d in Z_ORDER:
        pl.semaphore_signal(barrier, inc=1, device_id=zdev(d), device_id_type=MESH_IDS)
    for d in J_ORDER:
        pl.semaphore_signal(barrier, inc=1, device_id=jdev(d), device_id_type=MESH_IDS)
    for d in T_ORDER:
        pl.semaphore_signal(barrier, inc=1, device_id=tdev(d), device_id_type=MESH_IDS)

    inputs = [
        pltpu.make_async_copy(src, dst, in_sem.at[k])
        for k, (src, dst) in enumerate(
            (
                (tokens_in, tokens),
                (attn_gain_in, attn_gain),
                (wq_hbm, wq_in),
                (wk_hbm, wk_in),
                (wv_hbm, wv_in),
                (route_ids_in, route_ids),
                (route_weights_in, route_weights),
                (wo_hbm, wo_in),
                (ffn_gain_in, ffn_gain),
                (branch_gate_in, branch_gate),
            )
        )
    ]
    for copy in inputs:
        copy.start()
    kv_copies = []
    for s in range(0, 16, 2):
        kv_copies.append(
            pltpu.make_async_copy(
                keys_hbm.at[pl.ds(s, 2), 0], keys.at[pl.ds(s, 2)], kv_sem.at[s]
            )
        )
    for s in range(0, 16, 2):
        kv_copies.append(
            pltpu.make_async_copy(
                values_hbm.at[pl.ds(s, 2), 0], values.at[pl.ds(s, 2)], kv_sem.at[s + 1]
            )
        )
    for copy in kv_copies:
        copy.start()
    dense_col = pl.ds(pl.multiple_of(mj * 128, 128), 128)
    locals_ = [
        pltpu.make_async_copy(dgate_hbm, dgate.at[:, dense_col], local_sem.at[0]),
        pltpu.make_async_copy(dup_hbm, dup.at[:, dense_col], local_sem.at[1]),
        pltpu.make_async_copy(ddown_hbm, ddown.at[dense_col], local_sem.at[2]),
        pltpu.make_async_copy(egate_hbm.at[0], egate, local_sem.at[3]),
        pltpu.make_async_copy(eup_hbm.at[0], eup, local_sem.at[4]),
        pltpu.make_async_copy(edown_hbm.at[0], edown, local_sem.at[5]),
    ]
    for copy in locals_:
        copy.start()

    for copy in inputs[0:2]:
        copy.wait()
    tok = tokens[...].astype(F32)
    normed = (
        tok * lax.rsqrt(jnp.mean(tok * tok, axis=-1, keepdims=True) + norm_eps) * attn_gain[...]
    ).astype(BF)
    for z in range(NZ):
        nsend[z] = normed[:, 256 * z : 256 * (z + 1)]
    for copy in inputs[2:]:
        copy.wait()

    pl.semaphore_wait(barrier, NJ + NZ + NT - 3)

    def chunk_of(src, dst, k, lo, hi):
        return exchange(
            J_ORDER,
            lambda d: remote(
                src.at[:, lo:hi],
                dst.at[mj, :, lo:hi],
                j_send.at[k, d],
                j_recv.at[k, d],
                jdev(d),
            ),
        )

    c_wa = chunk_of(wq_in, wq, 0, 0, 256)
    c_n = exchange(
        Z_ORDER,
        lambda d: remote(
            nsend.at[zpeer(d)], nslab.at[mz], z_send.at[0, d], z_recv.at[0, d], zdev(d)
        ),
    )
    c_wb = chunk_of(wq_in, wq, 1, 256, 512)
    c_wk = chunk_of(wk_in, wk, 2, 0, 128)
    c_wv = chunk_of(wv_in, wv, 9, 0, 128)
    c_wo = exchange(
        J_ORDER, lambda d: remote(wo_in, wo.at[mj], j_send.at[3, d], j_recv.at[3, d], jdev(d))
    )
    c_dg = exchange(
        J_ORDER,
        lambda d: remote(
            dgate_hbm, dgate.at[:, dense_col], j_send.at[4, d], j_recv.at[4, d], jdev(d)
        ),
    )
    c_du = exchange(
        J_ORDER,
        lambda d: remote(
            dup_hbm, dup.at[:, dense_col], j_send.at[5, d], j_recv.at[5, d], jdev(d)
        ),
    )
    c_dd = exchange(
        J_ORDER,
        lambda d: remote(
            ddown_hbm, ddown.at[dense_col], j_send.at[6, d], j_recv.at[6, d], jdev(d)
        ),
    )
    wq[mj] = wq_in[...]
    wk[mj] = wk_in[...]
    wv[mj] = wv_in[...]
    wo[mj] = wo_in[...]
    nslab[mz] = nsend[mz]
    tok_all[mz] = tokens[...]

    row_expert = lax.shift_right_logical(iota((128, 16), 0), 1)
    named = jnp.zeros((128, 16), F32)
    weighed = jnp.zeros((128, 16), F32)
    for k in range(4):
        hit = route_ids[k : k + 1, :] == row_expert
        named = named + one_if(hit)
        weighed = weighed + jnp.where(hit, route_weights[k : k + 1, :], 0.0)
    earlier = one_if(iota((16, 16), 0) < iota((16, 16), 1)).astype(BF)
    rank = dot(named.astype(BF), earlier)
    row_rank = jnp.bitwise_and(iota((128, 16), 0), 1).astype(F32)
    slots = jnp.where(rank == row_rank, weighed, 0.0)
    wd_all[mz] = jnp.concatenate([slots, jnp.zeros((128, 112), F32)], axis=1).T[0:16]

    def q_chunk(k, weight, lo, hi, at):
        width = hi - lo
        cols = slice(at, at + width)
        qsend[:, :, cols] = (
            dot(nslab[...].reshape(128, 256), weight[:, :, lo:hi].reshape(256, width))
            .astype(BF)
            .reshape(NZ, 16, width)
        )

    def q_exchange(k, lo, hi):
        copies = exchange(
            Z_ORDER,
            lambda d: remote(
                qsend.at[zpeer(d), :, lo:hi],
                qrecv.at[mz, :, lo:hi],
                z_send.at[k, d],
                z_recv.at[k, d],
                zdev(d),
            ),
        )
        qrecv[mz, :, lo:hi] = qsend[mz, :, lo:hi]
        return copies

    def q_sum(lo, hi):
        total = qrecv[0, :, lo:hi].astype(F32)
        for z in range(1, NZ):
            total = total + qrecv[z, :, lo:hi].astype(F32)
        return total.astype(BF)

    arrived(c_n)
    arrived(c_wa)
    q_chunk(0, wq, 0, 256, 0)
    c_qa = q_exchange(1, 0, 256)
    arrived(c_wb)
    q_chunk(1, wq, 256, 512, 256)
    c_qb = q_exchange(2, 256, 512)
    arrived(c_wk)
    arrived(c_wv)
    q_chunk(2, wk, 0, 128, 512)
    q_chunk(2, wv, 0, 128, 640)
    c_qc = q_exchange(3, 512, 768)
    own_cols = pl.ds(pl.multiple_of(mt * 512, 512), 512)
    c_tok = exchange(
        Z_ORDER,
        lambda d: remote(
            tokens.at[:, own_cols],
            tok_all.at[mz, :, own_cols],
            z_send.at[4, d],
            z_recv.at[4, d],
            zdev(d),
        ),
    )
    c_wd = exchange(
        Z_ORDER,
        lambda d: remote(
            wd_all.at[mz], wd_all.at[mz], z_send.at[5, d], z_recv.at[5, d], zdev(d)
        ),
    )
    for copy in kv_copies:
        copy.wait()
    arrived(c_qa)
    total_a = q_sum(0, 256)
    arrived(c_qb)
    total_b = q_sum(256, 512)

    q_rows = jnp.zeros((64, 128), F32)
    for h in range(4):
        part = (total_a, total_b)[h // 2][:, 128 * (h % 2) : 128 * (h % 2 + 1)]
        spread = one_if(iota((64, 16), 0) == 4 * iota((64, 16), 1) + h).astype(BF)
        q_rows = q_rows + dot(spread, part)
    q64[...] = q_rows
    first = iota((8, 128), 0) < 4
    for p in range(8):
        q8 = q64[8 * p : 8 * p + 8]
        qa = jnp.where(first, q8, 0.0).astype(BF)
        qb = jnp.where(first, 0.0, q8).astype(BF)
        scores[8 * p : 8 * p + 8] = dot_nt(qa, keys[2 * p]) + dot_nt(qb, keys[2 * p + 1])

    c_ftok = []
    for copy, d in reversed(list(zip(c_tok, Z_ORDER))):
        copy.wait_recv()
        block = tok_all.at[zsource(d), :, own_cols]
        c_ftok += exchange(
            T_ORDER,
            lambda e: remote(block, block, ft_send.at[d, e], ft_recv.at[d, e], tdev(e)),
        )

    row = iota((64, 1), 0)
    head = jnp.bitwise_and(row, 3)
    seq = lax.shift_right_logical(row, 2)
    bias_col = jnp.zeros((64, 1), F32)
    for h in range(4):
        bias_col = jnp.where(head == h, bias[h], bias_col)
    len_col = jnp.zeros((64, 1), jnp.int32)
    for s in range(16):
        len_col = jnp.where(seq == s, lengths[s], len_col)
    after = one_if(iota((128, 128), 0) > iota((128, 128), 1)).astype(BF)
    carry = jnp.zeros((64, 1), F32)
    for b in reversed(range(8)):
        cols = slice(128 * b, 128 * (b + 1))
        zz = scores[:, cols] * (128 ** (-0.5)) + bias_col
        inside = (iota((64, 128), 1) + 128 * b) < len_col
        soft = jnp.log1p(jnp.exp(-jnp.abs(zz)))
        keep = jnp.where(inside, jnp.minimum(-zz, 0.0) - soft, 0.0)
        take = jnp.minimum(zz, 0.0) - soft
        k1 = keep.astype(BF)
        r1 = keep - k1.astype(F32)
        k2 = r1.astype(BF)
        k3 = (r1 - k2.astype(F32)).astype(BF)
        between = dot(k1, after) + dot(k2, after) + dot(k3, after) + carry
        carry = between[:, 0:1] + keep[:, 0:1]
        scores[:, cols] = jnp.where(inside, jnp.exp(take + between), 0.0)

    for p in range(8):
        w8 = scores[8 * p : 8 * p + 8].astype(BF)
        att64[8 * p : 8 * p + 8] = jnp.where(
            first, dot(w8, values[2 * p]), dot(w8, values[2 * p + 1])
        )
    att_rows = att64[...].astype(BF)
    for h in range(4):
        pick = one_if(iota((16, 64), 1) == 4 * iota((16, 64), 0) + h).astype(BF)
        att_all[mz, :, 128 * h : 128 * (h + 1)] = dot(pick, att_rows).astype(BF)

    c_a = exchange(
        Z_ORDER,
        lambda d: remote(
            att_all.at[mz], att_all.at[mz], z_send.at[6, d], z_recv.at[6, d], zdev(d)
        ),
    )
    arrived(c_qc)
    out[:, 512:768] = q_sum(512, 768)
    arrived(c_wd)
    slot_of_row = 16 * mz + 2 * lax.shift_right_logical(iota((128, 128), 0), 4)
    slot_of_row = slot_of_row + jnp.bitwise_and(iota((128, 128), 0), 1)
    spread = one_if(slot_of_row == iota((128, 128), 1)).astype(BF)
    row_z = jnp.bitwise_and(lax.shift_right_logical(iota((128, 128), 0), 1), 7)
    own_z = row_z == lax.shift_right_logical(iota((128, 128), 1), 4)
    wd = wd_all[...].reshape(128, 128)
    wd_hi = wd.astype(BF)
    wd_lo = (wd - wd_hi.astype(F32)).astype(BF)
    filled = one_if(wd > 0.0).astype(BF)
    dispatch = jnp.where(own_z, dot_nt(spread, filled), 0.0).astype(BF)
    row_z_t = jnp.bitwise_and(lax.shift_right_logical(iota((128, 128), 1), 1), 7)
    own_z_t = row_z_t == lax.shift_right_logical(iota((128, 128), 0), 4)
    comb_hi = jnp.where(own_z_t, dot_nt(wd_hi, spread), 0.0).astype(BF)
    comb_lo = jnp.where(own_z_t, dot_nt(wd_lo, spread), 0.0).astype(BF)
    arrived(c_wo)
    arrived(c_a)
    po_send[...] = (
        dot_nt(att_all[...].reshape(128, 512), wo[...].reshape(256, 512))
        .astype(BF)
        .reshape(NT, 32, 256)
    )
    c_po = exchange(
        T_ORDER,
        lambda d: remote(
            po_send.at[tpeer(d)], po_recv.at[mt], t_send.at[0, d], t_recv.at[0, d], tdev(d)
        ),
    )
    po_recv[mt] = po_send[mt]
    arrived(c_po)
    part = po_recv[0].astype(F32)
    for t in range(1, NT):
        part = part + po_recv[t].astype(F32)
    mixed[mt, mz] = part.astype(BF)

    own_block = mixed.at[mt, mz]
    c_mx = exchange(
        Z_ORDER,
        lambda d: remote(own_block, own_block, z_send.at[7, d], z_recv.at[7, d], zdev(d)),
    )
    c_fm = exchange(
        T_ORDER,
        lambda e: remote(own_block, own_block, fm_send.at[0, e], fm_recv.at[0, e], tdev(e)),
    )
    for copy, d in reversed(list(zip(c_mx, Z_ORDER))):
        copy.wait_recv()
        block = mixed.at[mt, zsource(d)]
        c_fm += exchange(
            T_ORDER,
            lambda e: remote(block, block, fm_send.at[d, e], fm_recv.at[d, e], tdev(e)),
        )
    for copy in c_ftok:
        copy.wait_recv()
    for copy in c_fm:
        copy.wait_recv()
    for z in range(NZ):
        pieces = []
        square = jnp.zeros((16, 1), F32)
        for s in range(NZ):
            cols = slice(256 * s, 256 * (s + 1))
            piece = tok_all[z, :, cols].astype(F32) + mixed[
                z // 2, s, 16 * (z % 2) : 16 * (z % 2) + 16
            ].astype(F32)
            square = square + jnp.sum(piece * piece, axis=-1, keepdims=True)
            pieces.append(piece)
        scale = lax.rsqrt(square * (1.0 / 2048) + norm_eps)
        for s in range(NZ):
            cols = slice(256 * s, 256 * (s + 1))
            xs[z, :, cols] = (pieces[s] * scale * ffn_gain[:, cols]).astype(BF)

    for b in range(4):
        cols = slice(512 * b, 512 * (b + 1))
        row_send[:, :, cols] = (
            dot(dispatch, xs[:, :, cols].reshape(128, 512)).astype(BF).reshape(NJ, 16, 512)
        )
    c_row = exchange(
        J_ORDER,
        lambda d: remote(
            row_send.at[jpeer(d)], row_recv.at[mj], j_send.at[7, d], j_recv.at[7, d], jdev(d)
        ),
    )
    row_recv[mj] = row_send[mj]

    for copy in locals_:
        copy.wait()
    arrived(c_dg)
    arrived(c_du)
    x_own = xs[:, :, own_cols].reshape(128, 512)
    for t in range(NT):
        cols = slice(256 * t, 256 * (t + 1))
        pd_send[t, :, 0:256] = dot(x_own, dgate[:, cols]).astype(BF)
        pd_send[t, :, 256:512] = dot(x_own, dup[:, cols]).astype(BF)
    c_pd = exchange(
        T_ORDER,
        lambda d: remote(
            pd_send.at[tpeer(d)], pd_recv.at[mt], t_send.at[1, d], t_recv.at[1, d], tdev(d)
        ),
    )
    pd_recv[mt] = pd_send[mt]
    weighted = jnp.zeros((128, 128), F32)
    for r in range(16):
        weighted = weighted + (
            xs[:, :, 128 * r : 128 * (r + 1)].reshape(128, 128).astype(F32)
            * branch_gate[r : r + 1, :].astype(F32)
        )
    branch = jax.nn.sigmoid(jnp.sum(weighted, axis=-1, keepdims=True))
    arrived(c_pd)
    pre = pd_recv[0].astype(F32)
    for t in range(1, NT):
        pre = pre + pd_recv[t].astype(F32)
    gate_d = pre[:, 0:256]
    hid[mt] = (gate_d * jax.nn.sigmoid(gate_d) * pre[:, 256:512]).astype(BF)
    c_h = exchange(
        T_ORDER,
        lambda d: remote(hid.at[mt], hid.at[mt], t_send.at[2, d], t_recv.at[2, d], tdev(d)),
    )

    arrived(c_row)
    rows = row_recv[...].reshape(128, 2048)
    gate_c = jnp.minimum(dot(rows, egate[...]), clamp_limit)
    up_c = jnp.clip(dot(rows, eup[...]), -clamp_limit, clamp_limit)
    unit = ((up_c + 1.0) * gate_c * jax.nn.sigmoid(swish_alpha * gate_c)).astype(BF)
    for t in range(NT):
        pe_send[t] = dot(unit, edown[:, 512 * t : 512 * (t + 1)]).astype(BF)
    c_pe = exchange(
        T_ORDER,
        lambda d: remote(
            pe_send.at[tpeer(d)], pe_recv.at[mt], t_send.at[3, d], t_recv.at[3, d], tdev(d)
        ),
    )
    pe_recv[mt] = pe_send[mt]

    arrived(c_h)
    arrived(c_dd)
    down = dot(hid[0], ddown[0:256])
    for t in range(1, NT):
        down = down + dot(hid[t], ddown[256 * t : 256 * (t + 1)])
    dense_part[...] = down * branch

    arrived(c_pe)
    total_e = pe_recv[0].astype(F32)
    for t in range(1, NT):
        total_e = total_e + pe_recv[t].astype(F32)
    er[...] = total_e.astype(BF).reshape(NJ, 16, 512)
    c_er = exchange(
        J_ORDER,
        lambda d: remote(
            er.at[jpeer(d)], er_recv.at[mj], j_send.at[8, d], j_recv.at[8, d], jdev(d)
        ),
    )
    er_recv[mj] = er[mj]
    arrived(c_er)
    back = er_recv[...].reshape(128, 512)
    fin_send[...] = (
        (dot(comb_hi, back) + dot(comb_lo, back) + dense_part[...]).astype(BF).reshape(NZ, 16, 512)
    )
    c_f = exchange(
        Z_ORDER,
        lambda d: remote(
            fin_send.at[zpeer(d)], fin_recv.at[mz], z_send.at[8, d], z_recv.at[8, d], zdev(d)
        ),
    )
    fin_recv[mz] = fin_send[mz]
    quarter = lax.div(mz, 2)
    own_rows = pl.ds(pl.multiple_of(lax.rem(mz, 2) * 16, 16), 16)
    final = tokens[:, own_cols].astype(F32) + jnp.concatenate(
        [mixed[quarter, 2 * mt, own_rows], mixed[quarter, 2 * mt + 1, own_rows]], axis=1
    ).astype(F32)
    arrived(c_f)
    for z in range(NZ):
        final = final + fin_recv[z].astype(F32)
    out[:, 0:512] = final.astype(BF)

    for copy in started:
        copy.wait_send()


def split_kernel(both, layer_out, new_keys, new_values):
    layer_out[...] = both[:, 0:512]
    new_keys[...] = both[:, 512:640]
    new_values[...] = both[:, 640:768]


def body(
    tokens,
    attn_gain,
    query_weight,
    key_weight,
    value_weight,
    break_bias,
    cache_keys,
    cache_values,
    lengths,
    out_weight,
    ffn_gain,
    branch_gate,
    dense_gate,
    dense_up,
    dense_down,
    route_ids,
    route_weights,
    expert_gate,
    expert_up,
    expert_down,
):
    vm = pl.BlockSpec(memory_space=pltpu.VMEM)
    sm = pl.BlockSpec(memory_space=pltpu.SMEM)
    hbm = pl.BlockSpec(memory_space=pl.ANY)
    V = pltpu.VMEM
    D = pltpu.SemaphoreType.DMA
    both = pl.pallas_call(
        kernel,
        name="layer",
        out_shape=jax.ShapeDtypeStruct((16, 768), BF),
        in_specs=[hbm] * 5 + [sm, hbm, hbm, sm] + [hbm] * 11,
        out_specs=vm,
        scratch_shapes=[
            V((16, 2048), BF),
            V((1, 2048), F32),
            V((32, 512), BF),
            V((32, 128), BF),
            V((32, 128), BF),
            V((32, 512), BF),
            V((1, 2048), F32),
            V((16, 128), BF),
            V((4, 16), jnp.int32),
            V((4, 16), F32),
            V((16, 1024, 128), BF),
            V((16, 1024, 128), BF),
            V((2048, 256), BF),
            V((2048, 256), BF),
            V((256, 2048), BF),
            V((512, 1024), BF),
            V((512, 1024), BF),
            V((1024, 512), BF),
            V((NJ, 32, 512), BF),
            V((NJ, 32, 128), BF),
            V((NJ, 32, 128), BF),
            V((NJ, 32, 512), BF),
            V((NZ, 16, 256), BF),
            V((NZ, 16, 256), BF),
            V((NZ, 16, 768), BF),
            V((NZ, 16, 768), BF),
            V((64, 1024), F32),
            V((64, 128), F32),
            V((64, 128), F32),
            V((NZ, 16, 512), BF),
            V((NZ, 16, 128), F32),
            V((NZ, 16, 2048), BF),
            V((NT, 32, 256), BF),
            V((NT, 32, 256), BF),
            V((NT, NZ, 32, 256), BF),
            V((NZ, 16, 2048), BF),
            V((NJ, 16, 2048), BF),
            V((NJ, 16, 2048), BF),
            V((NT, 128, 512), BF),
            V((NT, 128, 512), BF),
            V((NT, 128, 256), BF),
            V((NT, 128, 512), BF),
            V((NT, 128, 512), BF),
            V((NJ, 16, 512), BF),
            V((NJ, 16, 512), BF),
            V((128, 512), F32),
            V((NZ, 16, 512), BF),
            V((NZ, 16, 512), BF),
            D((10,)),
            D((6,)),
            D((16,)),
            D((9, NZ)),
            D((9, NZ)),
            D((10, NJ)),
            D((10, NJ)),
            D((4, NT)),
            D((4, NT)),
            D((NZ, NT)),
            D((NZ, NT)),
            D((NZ, NT)),
            D((NZ, NT)),
        ],
        compiler_params=pltpu.CompilerParams(
            collective_id=0,
            has_side_effects=True,
            vmem_limit_bytes=60 * 1024 * 1024,
        ),
    )(
        tokens,
        attn_gain.reshape(1, -1),
        query_weight,
        key_weight,
        value_weight,
        break_bias,
        cache_keys,
        cache_values,
        lengths,
        out_weight.T,
        ffn_gain.reshape(1, -1),
        branch_gate.reshape(16, 128),
        dense_gate,
        dense_up,
        dense_down,
        route_ids.T,
        route_weights.T,
        expert_gate,
        expert_up,
        expert_down,
    )
    return tuple(
        pl.pallas_call(
            split_kernel,
            name="split",
            out_shape=(
                jax.ShapeDtypeStruct((16, 512), BF),
                jax.ShapeDtypeStruct((16, 128), BF),
                jax.ShapeDtypeStruct((16, 128), BF),
            ),
            in_specs=[vm],
            out_specs=(vm, vm, vm),
        )(both)
    )


def solution(mesh):
    split = Mesh(mesh.devices.reshape(NZ, NX, NC, NT), ("z", "x", "c", "tp"))
    return jax.shard_map(
        body,
        mesh=split,
        in_specs=(
            P(EP, None),
            P(),
            P(EP, "tp"),
            P(EP, "tp"),
            P(EP, "tp"),
            P("tp"),
            P(EP, "tp", None, None),
            P(EP, "tp", None, None),
            P(EP),
            P("tp", EP),
            P(),
            P(),
            P("tp", EP),
            P("tp", EP),
            P(EP, "tp"),
            P(EP, None),
            P(EP, None),
            P(EP, None, "tp"),
            P(EP, None, "tp"),
            P(EP, "tp", None),
        ),
        out_specs=(P(EP, "tp"), P(EP, "tp"), P(EP, "tp")),
        check_vma=False,
    )
```

time: 96.7 us -> 85.2 us (0.88)
  local copies, waits for them, and re-layouts: 6.56 us -> 0 us
  Pallas kernels: 87.8 us -> 84.4 us
  other arithmetic: 1.29 us -> 0 us
    unnamed x5 -> x0, local copies, waits for them, and re-layouts: 6.56 us -> none
    pallas_call x1 -> x2, Pallas kernels: 87.8 us -> 84.4 us  [the longest x1 83.1 us: body(): pl.pallas_call(kernel, name='layer', out_shape=jax.ShapeDtypeStruct((16,...]
    reshape x1 -> x0, other arithmetic: 1.29 us -> none  [body(): branch_gate.astype(F32).reshape(1, -1)]
where the time goes in v2:
time: 85.2 us; the launch traced here: 85.1 us
  Pallas kernels  84.4 us (99%)
    pallas_call x1, Pallas kernels, body(): pl.pallas_call(kernel, name='layer', out_shape=jax.ShapeDtypeStruct((16,...  83.1 us

profile of v2, /device:TPU:1, one launch (start us, length us, event | category | flops | bytes accessed | tf_op | source)
XLA Modules:
  0.0 85.1 jit_solution(1172259757081812088)
XLA Ops:
  0.6 83.1 %layer.1.both = bf16[16,768]{1,0:T(8,128)(2,1)} custom-call(bf16[16,2048]{1,0:T(8,128)(2,1)} %tokens_in.1, f32[1,2048]{1,0:T(1,128)} %bitcast.7, bf16[32,512]{1,0:T(8,128)(2,1)} %wq_hbm.1, bf16[32,128]{1,0:T(8,128)(2,1)} %wk_hbm.1, bf16[32,128]{1,0:T(8,128)(2,1)} %wv_hbm.1, f32[4]{0:T(128)} %bias.1, bf16[16,1,1024,128]{3,2,1,0:T(8,128)(2,1)} %keys_hbm.1, ...), custom_call_target="tpu_custom_call" | custom-call | tf_op jit(solution)/shard_map/layer/pallas_call | solution.py:651
  83.7 1.4 %split.1 = (bf16[16,512]{1,0:T(8,128)(2,1)}, bf16[16,128]{1,0:T(8,128)(2,1)}, bf16[16,128]{1,0:T(8,128)(2,1)}) custom-call(bf16[16,768]{1,0:T(8,128)(2,1)} %layer.1.both), custom_call_target="tpu_custom_call" | custom-call | tf_op jit(solution)/shard_map/split/pallas_call | solution.py:748

commit v3 on v2

--- a/solution.py
+++ b/solution.py
@@ -125,6 +125,8 @@
     ft_recv,
     fm_send,
     fm_recv,
+    p_send,
+    p_recv,
 ):
     mz = lax.axis_index("z")
     mxx = lax.axis_index("x")
@@ -263,30 +265,43 @@
             nsend.at[zpeer(d)], nslab.at[mz], z_send.at[0, d], z_recv.at[0, d], zdev(d)
         ),
     )
+    own_cols = pl.ds(pl.multiple_of(mt * 512, 512), 512)
+    c_tok = exchange(
+        Z_ORDER,
+        lambda d: remote(
+            tokens.at[:, own_cols],
+            tok_all.at[mz, :, own_cols],
+            z_send.at[4, d],
+            z_recv.at[4, d],
+            zdev(d),
+        ),
+    )
     c_wb = chunk_of(wq_in, wq, 1, 256, 512)
     c_wk = chunk_of(wk_in, wk, 2, 0, 128)
     c_wv = chunk_of(wv_in, wv, 9, 0, 128)
     c_wo = exchange(
         J_ORDER, lambda d: remote(wo_in, wo.at[mj], j_send.at[3, d], j_recv.at[3, d], jdev(d))
     )
-    c_dg = exchange(
-        J_ORDER,
-        lambda d: remote(
-            dgate_hbm, dgate.at[:, dense_col], j_send.at[4, d], j_recv.at[4, d], jdev(d)
-        ),
-    )
-    c_du = exchange(
-        J_ORDER,
-        lambda d: remote(
-            dup_hbm, dup.at[:, dense_col], j_send.at[5, d], j_recv.at[5, d], jdev(d)
-        ),
-    )
-    c_dd = exchange(
-        J_ORDER,
-        lambda d: remote(
-            ddown_hbm, ddown.at[dense_col], j_send.at[6, d], j_recv.at[6, d], jdev(d)
-        ),
-    )
+    dense = (
+        (dgate_hbm, lambda j: dgate.at[:, pl.ds(pl.multiple_of(j * 128, 128), 128)]),
+        (dup_hbm, lambda j: dup.at[:, pl.ds(pl.multiple_of(j * 128, 128), 128)]),
+        (ddown_hbm, lambda j: ddown.at[pl.ds(pl.multiple_of(j * 128, 128), 128)]),
+    )
+    c_dx = [
+        exchange(
+            (4, 2, 6),
+            lambda d: remote(src, part(mj), j_send.at[4 + k, d], j_recv.at[4 + k, d], jdev(d)),
+        )
+        for k, (src, part) in enumerate(dense)
+    ]
+    partner = {"c": 1 - mc}
+    c_dp = [
+        exchange(
+            (0,),
+            lambda d: remote(src, part(mj), p_send.at[k, d], p_recv.at[k, d], partner),
+        )
+        for k, (src, part) in enumerate(dense)
+    ]
     wq[mj] = wq_in[...]
     wk[mj] = wk_in[...]
     wv[mj] = wv_in[...]
@@ -348,23 +363,21 @@
     q_chunk(2, wk, 0, 128, 512)
     q_chunk(2, wv, 0, 128, 640)
     c_qc = q_exchange(3, 512, 768)
-    own_cols = pl.ds(pl.multiple_of(mt * 512, 512), 512)
-    c_tok = exchange(
-        Z_ORDER,
-        lambda d: remote(
-            tokens.at[:, own_cols],
-            tok_all.at[mz, :, own_cols],
-            z_send.at[4, d],
-            z_recv.at[4, d],
-            zdev(d),
-        ),
-    )
     c_wd = exchange(
         Z_ORDER,
         lambda d: remote(
             wd_all.at[mz], wd_all.at[mz], z_send.at[5, d], z_recv.at[5, d], zdev(d)
         ),
     )
+    c_ftok = []
+    for copy, d in reversed(list(zip(c_tok, Z_ORDER))):
+        copy.wait_recv()
+        block = tok_all.at[zsource(d), :, own_cols]
+        c_ftok += exchange(
+            T_ORDER,
+            lambda e: remote(block, block, ft_send.at[d, e], ft_recv.at[d, e], tdev(e)),
+        )
+
     for copy in kv_copies:
         copy.wait()
     arrived(c_qa)
@@ -384,15 +397,6 @@
         qa = jnp.where(first, q8, 0.0).astype(BF)
         qb = jnp.where(first, 0.0, q8).astype(BF)
         scores[8 * p : 8 * p + 8] = dot_nt(qa, keys[2 * p]) + dot_nt(qb, keys[2 * p + 1])
-
-    c_ftok = []
-    for copy, d in reversed(list(zip(c_tok, Z_ORDER))):
-        copy.wait_recv()
-        block = tok_all.at[zsource(d), :, own_cols]
-        c_ftok += exchange(
-            T_ORDER,
-            lambda e: remote(block, block, ft_send.at[d, e], ft_recv.at[d, e], tdev(e)),
-        )
 
     row = iota((64, 1), 0)
     head = jnp.bitwise_and(row, 3)
@@ -482,6 +486,18 @@
         T_ORDER,
         lambda e: remote(own_block, own_block, fm_send.at[0, e], fm_recv.at[0, e], tdev(e)),
     )
+    for k, (src, part) in enumerate(dense):
+        arrived(c_dx[k])
+        c_dp[k] += exchange(
+            (2, 4, 6),
+            lambda d: remote(
+                part(lax.rem(mj + NJ - d, NJ)),
+                part(lax.rem(mj + NJ - d, NJ)),
+                p_send.at[k, d // 2],
+                p_recv.at[k, d // 2],
+                partner,
+            ),
+        )
     for copy, d in reversed(list(zip(c_mx, Z_ORDER))):
         copy.wait_recv()
         block = mixed.at[mt, zsource(d)]
@@ -523,8 +539,8 @@
 
     for copy in locals_:
         copy.wait()
-    arrived(c_dg)
-    arrived(c_du)
+    arrived(c_dp[0])
+    arrived(c_dp[1])
     x_own = xs[:, :, own_cols].reshape(128, 512)
     for t in range(NT):
         cols = slice(256 * t, 256 * (t + 1))
@@ -571,7 +587,7 @@
     pe_recv[mt] = pe_send[mt]
 
     arrived(c_h)
-    arrived(c_dd)
+    arrived(c_dp[2])
     down = dot(hid[0], ddown[0:256])
     for t in range(1, NT):
         down = down + dot(hid[t], ddown[256 * t : 256 * (t + 1)])
@@ -716,6 +732,8 @@
             D((NZ, NT)),
             D((NZ, NT)),
             D((NZ, NT)),
+            D((3, 4)),
+            D((3, 4)),
         ],
         compiler_params=pltpu.CompilerParams(
             collective_id=0,

time: 85.2 us -> 78.5 us (0.921)
  Pallas kernels: 84.4 us -> 77.7 us
    pallas_call x1, Pallas kernels: 83.1 us -> 76.3 us  [body(): pl.pallas_call(kernel, name='layer', out_shape=jax.ShapeDtypeStruct((16,...]
where the time goes in v3:
time: 78.5 us; the launch traced here: 78.3 us
  Pallas kernels  77.7 us (99%)
    pallas_call x1, Pallas kernels, body(): pl.pallas_call(kernel, name='layer', out_shape=jax.ShapeDtypeStruct((16,...  76.3 us

profile of v3, /device:TPU:1, one launch (start us, length us, event | category | flops | bytes accessed | tf_op | source)
XLA Modules:
  0.0 78.3 jit_solution(13703229187508861888)
XLA Ops:
  0.6 76.3 %layer.1.both = bf16[16,768]{1,0:T(8,128)(2,1)} custom-call(bf16[16,2048]{1,0:T(8,128)(2,1)} %tokens_in.1, f32[1,2048]{1,0:T(1,128)} %bitcast.7, bf16[32,512]{1,0:T(8,128)(2,1)} %wq_hbm.1, bf16[32,128]{1,0:T(8,128)(2,1)} %wk_hbm.1, bf16[32,128]{1,0:T(8,128)(2,1)} %wv_hbm.1, f32[4]{0:T(128)} %bias.1, bf16[16,1,1024,128]{3,2,1,0:T(8,128)(2,1)} %keys_hbm.1, ...), custom_call_target="tpu_custom_call" | custom-call | tf_op jit(solution)/shard_map/layer/pallas_call | solution.py:667
  77.0 1.4 %split.1 = (bf16[16,512]{1,0:T(8,128)(2,1)}, bf16[16,128]{1,0:T(8,128)(2,1)}, bf16[16,128]{1,0:T(8,128)(2,1)}) custom-call(bf16[16,768]{1,0:T(8,128)(2,1)} %layer.1.both), custom_call_target="tpu_custom_call" | custom-call | tf_op jit(solution)/shard_map/split/pallas_call | solution.py:766

commit v4 on v3

--- a/solution.py
+++ b/solution.py
@@ -40,6 +40,7 @@
 Z_ORDER = (4, 3, 5, 2, 6, 1, 7)
 J_ORDER = (4, 3, 5, 2, 6, 1, 7)
 T_ORDER = (2, 1, 3)
+HALVES = ((0, 1, 2, 6), (4, 5, 3, 7))
 
 
 def kernel(
@@ -48,10 +49,10 @@
     wq_hbm,
     wk_hbm,
     wv_hbm,
-    bias,
+    bias_hbm,
     keys_hbm,
     values_hbm,
-    lengths,
+    lengths_hbm,
     wo_hbm,
     ffn_gain_in,
     branch_gate_in,
@@ -74,6 +75,8 @@
     branch_gate,
     route_ids,
     route_weights,
+    bias,
+    lengths,
     keys,
     values,
     egate,
@@ -153,6 +156,14 @@
         j = jpeer(d)
         return {"x": lax.div(j, NC), "c": lax.rem(j, NC)}
 
+    def away(k):
+        x = lax.rem(mxx + k // 2, NX)
+        c = lax.rem(mc + k % 2, NC)
+        return x * NC + c, {"x": x, "c": c}
+
+    def back_to(k):
+        return {"x": lax.rem(mxx + NX - k // 2, NX), "c": lax.rem(mc + k % 2, NC)}
+
     def tdev(d):
         return {"tp": tpeer(d)}
 
@@ -201,6 +212,8 @@
                 (wo_hbm, wo_in),
                 (ffn_gain_in, ffn_gain),
                 (branch_gate_in, branch_gate),
+                (bias_hbm, bias),
+                (lengths_hbm, lengths),
             )
         )
     ]
@@ -529,13 +542,21 @@
         row_send[:, :, cols] = (
             dot(dispatch, xs[:, :, cols].reshape(128, 512)).astype(BF).reshape(NJ, 16, 512)
         )
-    c_row = exchange(
-        J_ORDER,
-        lambda d: remote(
-            row_send.at[jpeer(d)], row_recv.at[mj], j_send.at[7, d], j_recv.at[7, d], jdev(d)
-        ),
-    )
-    row_recv[mj] = row_send[mj]
+    c_row = []
+    for half, order in enumerate(((2, 6, 1), (4, 5, 3, 7))):
+        c_row.append(
+            exchange(
+                order,
+                lambda k: remote(
+                    row_send.at[away(k)[0]],
+                    row_recv.at[4 * half + HALVES[half].index(k)],
+                    j_send.at[7, k],
+                    j_recv.at[7, k],
+                    away(k)[1],
+                ),
+            )
+        )
+    row_recv[0] = row_send[mj]
 
     for copy in locals_:
         copy.wait()
@@ -560,6 +581,29 @@
             * branch_gate[r : r + 1, :].astype(F32)
         )
     branch = jax.nn.sigmoid(jnp.sum(weighted, axis=-1, keepdims=True))
+    c_pe = []
+    for half in range(2):
+        arrived(c_row[half])
+        rows = row_recv[4 * half : 4 * half + 4].reshape(64, 2048)
+        gate_c = jnp.minimum(dot(rows, egate[...]), clamp_limit)
+        up_c = jnp.clip(dot(rows, eup[...]), -clamp_limit, clamp_limit)
+        unit = ((up_c + 1.0) * gate_c * jax.nn.sigmoid(swish_alpha * gate_c)).astype(BF)
+        for t in range(NT):
+            pe_send[half, t] = dot(unit, edown[:, 512 * t : 512 * (t + 1)]).astype(BF)
+        c_pe.append(
+            exchange(
+                T_ORDER,
+                lambda d: remote(
+                    pe_send.at[half, tpeer(d)],
+                    pe_recv.at[half, mt],
+                    t_send.at[3 + half, d],
+                    t_recv.at[3 + half, d],
+                    tdev(d),
+                ),
+            )
+        )
+        pe_recv[half, mt] = pe_send[half, mt]
+
     arrived(c_pd)
     pre = pd_recv[0].astype(F32)
     for t in range(1, NT):
@@ -571,20 +615,24 @@
         lambda d: remote(hid.at[mt], hid.at[mt], t_send.at[2, d], t_recv.at[2, d], tdev(d)),
     )
 
-    arrived(c_row)
-    rows = row_recv[...].reshape(128, 2048)
-    gate_c = jnp.minimum(dot(rows, egate[...]), clamp_limit)
-    up_c = jnp.clip(dot(rows, eup[...]), -clamp_limit, clamp_limit)
-    unit = ((up_c + 1.0) * gate_c * jax.nn.sigmoid(swish_alpha * gate_c)).astype(BF)
-    for t in range(NT):
-        pe_send[t] = dot(unit, edown[:, 512 * t : 512 * (t + 1)]).astype(BF)
-    c_pe = exchange(
-        T_ORDER,
-        lambda d: remote(
-            pe_send.at[tpeer(d)], pe_recv.at[mt], t_send.at[3, d], t_recv.at[3, d], tdev(d)
-        ),
-    )
-    pe_recv[mt] = pe_send[mt]
+    c_er = []
+    for half in range(2):
+        arrived(c_pe[half])
+        total_e = pe_recv[half, 0].astype(F32)
+        for t in range(1, NT):
+            total_e = total_e + pe_recv[half, t].astype(F32)
+        er[4 * half : 4 * half + 4] = total_e.astype(BF).reshape(4, 16, 512)
+        c_er += exchange(
+            ((2, 6, 1), (4, 5, 3, 7))[half],
+            lambda k: remote(
+                er.at[4 * half + HALVES[half].index(k)],
+                er_recv.at[mj],
+                j_send.at[8, k],
+                j_recv.at[8, k],
+                back_to(k),
+            ),
+        )
+    er_recv[mj] = er[0]
 
     arrived(c_h)
     arrived(c_dp[2])
@@ -593,18 +641,6 @@
         down = down + dot(hid[t], ddown[256 * t : 256 * (t + 1)])
     dense_part[...] = down * branch
 
-    arrived(c_pe)
-    total_e = pe_recv[0].astype(F32)
-    for t in range(1, NT):
-        total_e = total_e + pe_recv[t].astype(F32)
-    er[...] = total_e.astype(BF).reshape(NJ, 16, 512)
-    c_er = exchange(
-        J_ORDER,
-        lambda d: remote(
-            er.at[jpeer(d)], er_recv.at[mj], j_send.at[8, d], j_recv.at[8, d], jdev(d)
-        ),
-    )
-    er_recv[mj] = er[mj]
     arrived(c_er)
     back = er_recv[...].reshape(128, 512)
     fin_send[...] = (
@@ -660,7 +696,6 @@
     expert_down,
 ):
     vm = pl.BlockSpec(memory_space=pltpu.VMEM)
-    sm = pl.BlockSpec(memory_space=pltpu.SMEM)
     hbm = pl.BlockSpec(memory_space=pl.ANY)
     V = pltpu.VMEM
     D = pltpu.SemaphoreType.DMA
@@ -668,7 +703,7 @@
         kernel,
         name="layer",
         out_shape=jax.ShapeDtypeStruct((16, 768), BF),
-        in_specs=[hbm] * 5 + [sm, hbm, hbm, sm] + [hbm] * 11,
+        in_specs=[hbm] * 20,
         out_specs=vm,
         scratch_shapes=[
             V((16, 2048), BF),
@@ -681,6 +716,8 @@
             V((16, 128), BF),
             V((4, 16), jnp.int32),
             V((4, 16), F32),
+            pltpu.SMEM((4,), F32),
+            pltpu.SMEM((16,), jnp.int32),
             V((16, 1024, 128), BF),
             V((16, 1024, 128), BF),
             V((2048, 256), BF),
@@ -712,22 +749,22 @@
             V((NT, 128, 512), BF),
             V((NT, 128, 512), BF),
             V((NT, 128, 256), BF),
-            V((NT, 128, 512), BF),
-            V((NT, 128, 512), BF),
+            V((2, NT, 64, 512), BF),
+            V((2, NT, 64, 512), BF),
             V((NJ, 16, 512), BF),
             V((NJ, 16, 512), BF),
             V((128, 512), F32),
             V((NZ, 16, 512), BF),
             V((NZ, 16, 512), BF),
-            D((10,)),
+            D((12,)),
             D((6,)),
             D((16,)),
             D((9, NZ)),
             D((9, NZ)),
             D((10, NJ)),
             D((10, NJ)),
-            D((4, NT)),
-            D((4, NT)),
+            D((5, NT)),
+            D((5, NT)),
             D((NZ, NT)),
             D((NZ, NT)),
             D((NZ, NT)),

time: 78.5 us -> 75 us (0.955)
  Pallas kernels: 77.7 us -> 74.2 us
    pallas_call x1, Pallas kernels: 76.3 us -> 72.9 us  [body(): pl.pallas_call(kernel, name='layer', out_shape=jax.ShapeDtypeStruct((16,...]
where the time goes in v4:
time: 75 us; the launch traced here: 74.9 us
  Pallas kernels  74.2 us (99%)
    pallas_call x1, Pallas kernels, body(): pl.pallas_call(kernel, name='layer', out_shape=jax.ShapeDtypeStruct((16,...  72.9 us

profile of v4, /device:TPU:1, one launch (start us, length us, event | category | flops | bytes accessed | tf_op | source)
XLA Modules:
  0.0 74.9 jit_solution(2339234454587867813)
XLA Ops:
  0.6 72.9 %layer.1.both = bf16[16,768]{1,0:T(8,128)(2,1)} custom-call(bf16[16,2048]{1,0:T(8,128)(2,1)} %tokens_in.1, f32[1,2048]{1,0:T(1,128)} %bitcast.7, bf16[32,512]{1,0:T(8,128)(2,1)} %wq_hbm.1, bf16[32,128]{1,0:T(8,128)(2,1)} %wk_hbm.1, bf16[32,128]{1,0:T(8,128)(2,1)} %wv_hbm.1, f32[4]{0:T(128)} %bias_hbm.1, bf16[16,1,1024,128]{3,2,1,0:T(8,128)(2,1)} %keys_hbm.1, ...), custom_call_target="tpu_custom_call" | custom-call | tf_op jit(solution)/shard_map/layer/pallas_call | solution.py:702
  73.5 1.4 %split.1 = (bf16[16,512]{1,0:T(8,128)(2,1)}, bf16[16,128]{1,0:T(8,128)(2,1)}, bf16[16,128]{1,0:T(8,128)(2,1)}) custom-call(bf16[16,768]{1,0:T(8,128)(2,1)} %layer.1.both), custom_call_target="tpu_custom_call" | custom-call | tf_op jit(solution)/shard_map/split/pallas_call | solution.py:803

commit v5 on v4

--- a/solution.py
+++ b/solution.py
@@ -246,16 +246,7 @@
     for copy in locals_:
         copy.start()
 
-    for copy in inputs[0:2]:
-        copy.wait()
-    tok = tokens[...].astype(F32)
-    normed = (
-        tok * lax.rsqrt(jnp.mean(tok * tok, axis=-1, keepdims=True) + norm_eps) * attn_gain[...]
-    ).astype(BF)
-    for z in range(NZ):
-        nsend[z] = normed[:, 256 * z : 256 * (z + 1)]
-    for copy in inputs[2:]:
-        copy.wait()
+    inputs[2].wait()
 
     pl.semaphore_wait(barrier, NJ + NZ + NT - 3)
 
@@ -272,6 +263,14 @@
         )
 
     c_wa = chunk_of(wq_in, wq, 0, 0, 256)
+    for copy in inputs[0:2]:
+        copy.wait()
+    tok = tokens[...].astype(F32)
+    normed = (
+        tok * lax.rsqrt(jnp.mean(tok * tok, axis=-1, keepdims=True) + norm_eps) * attn_gain[...]
+    ).astype(BF)
+    for z in range(NZ):
+        nsend[z] = normed[:, 256 * z : 256 * (z + 1)]
     c_n = exchange(
         Z_ORDER,
         lambda d: remote(
@@ -290,6 +289,8 @@
         ),
     )
     c_wb = chunk_of(wq_in, wq, 1, 256, 512)
+    for copy in inputs[3:]:
+        copy.wait()
     c_wk = chunk_of(wk_in, wk, 2, 0, 128)
     c_wv = chunk_of(wv_in, wv, 9, 0, 128)
     c_wo = exchange(
@@ -499,6 +500,13 @@
         T_ORDER,
         lambda e: remote(own_block, own_block, fm_send.at[0, e], fm_recv.at[0, e], tdev(e)),
     )
+    for copy, d in reversed(list(zip(c_mx, Z_ORDER))):
+        copy.wait_recv()
+        block = mixed.at[mt, zsource(d)]
+        c_fm += exchange(
+            T_ORDER,
+            lambda e: remote(block, block, fm_send.at[d, e], fm_recv.at[d, e], tdev(e)),
+        )
     for k, (src, part) in enumerate(dense):
         arrived(c_dx[k])
         c_dp[k] += exchange(
@@ -510,13 +518,6 @@
                 p_recv.at[k, d // 2],
                 partner,
             ),
-        )
-    for copy, d in reversed(list(zip(c_mx, Z_ORDER))):
-        copy.wait_recv()
-        block = mixed.at[mt, zsource(d)]
-        c_fm += exchange(
-            T_ORDER,
-            lambda e: remote(block, block, fm_send.at[d, e], fm_recv.at[d, e], tdev(e)),
         )
     for copy in c_ftok:
         copy.wait_recv()
@@ -537,6 +538,26 @@
             cols = slice(256 * s, 256 * (s + 1))
             xs[z, :, cols] = (pieces[s] * scale * ffn_gain[:, cols]).astype(BF)
 
+    for copy in locals_:
+        copy.wait()
+    arrived(c_dp[0])
+    arrived(c_dp[1])
+    x_own = xs[:, :, own_cols].reshape(128, 512)
+    c_pd = []
+    for d in T_ORDER + (0,):
+        to = tpeer(d)
+        cols = pl.ds(pl.multiple_of(to * 256, 256), 256)
+        block = pd_recv if d == 0 else pd_send
+        block[to, :, 0:256] = dot(x_own, dgate[:, cols]).astype(BF)
+        block[to, :, 256:512] = dot(x_own, dup[:, cols]).astype(BF)
+        if d > 0:
+            c_pd += exchange(
+                (d,),
+                lambda d: remote(
+                    pd_send.at[to], pd_recv.at[mt], t_send.at[1, d], t_recv.at[1, d], tdev(d)
+                ),
+            )
+
     for b in range(4):
         cols = slice(512 * b, 512 * (b + 1))
         row_send[:, :, cols] = (
@@ -558,22 +579,6 @@
         )
     row_recv[0] = row_send[mj]
 
-    for copy in locals_:
-        copy.wait()
-    arrived(c_dp[0])
-    arrived(c_dp[1])
-    x_own = xs[:, :, own_cols].reshape(128, 512)
-    for t in range(NT):
-        cols = slice(256 * t, 256 * (t + 1))
-        pd_send[t, :, 0:256] = dot(x_own, dgate[:, cols]).astype(BF)
-        pd_send[t, :, 256:512] = dot(x_own, dup[:, cols]).astype(BF)
-    c_pd = exchange(
-        T_ORDER,
-        lambda d: remote(
-            pd_send.at[tpeer(d)], pd_recv.at[mt], t_send.at[1, d], t_recv.at[1, d], tdev(d)
-        ),
-    )
-    pd_recv[mt] = pd_send[mt]
     weighted = jnp.zeros((128, 128), F32)
     for r in range(16):
         weighted = weighted + (
@@ -658,12 +663,14 @@
     final = tokens[:, own_cols].astype(F32) + jnp.concatenate(
         [mixed[quarter, 2 * mt, own_rows], mixed[quarter, 2 * mt + 1, own_rows]], axis=1
     ).astype(F32)
+    for copy in started[: -len(c_f)]:
+        copy.wait_send()
     arrived(c_f)
     for z in range(NZ):
         final = final + fin_recv[z].astype(F32)
     out[:, 0:512] = final.astype(BF)
 
-    for copy in started:
+    for copy in c_f:
         copy.wait_send()
 
 

time: 75 us -> 74.9 us (level)
  no operation moved by 1% of the time
where the time goes in v5:
time: 74.9 us; the launch traced here: 74.8 us
  Pallas kernels  74.2 us (99%)
    pallas_call x1, Pallas kernels, body(): pl.pallas_call(kernel, name='layer', out_shape=jax.ShapeDtypeStruct((16,...  72.8 us

profile of v5, /device:TPU:1, one launch (start us, length us, event | category | flops | bytes accessed | tf_op | source)
XLA Modules:
  0.0 74.8 jit_solution(3903871945369788295)
XLA Ops:
  0.6 72.8 %layer.1.both = bf16[16,768]{1,0:T(8,128)(2,1)} custom-call(bf16[16,2048]{1,0:T(8,128)(2,1)} %tokens_in.1, f32[1,2048]{1,0:T(1,128)} %bitcast.7, bf16[32,512]{1,0:T(8,128)(2,1)} %wq_hbm.1, bf16[32,128]{1,0:T(8,128)(2,1)} %wk_hbm.1, bf16[32,128]{1,0:T(8,128)(2,1)} %wv_hbm.1, f32[4]{0:T(128)} %bias_hbm.1, bf16[16,1,1024,128]{3,2,1,0:T(8,128)(2,1)} %keys_hbm.1, ...), custom_call_target="tpu_custom_call" | custom-call | tf_op jit(solution)/shard_map/layer/pallas_call | solution.py:709
  73.5 1.4 %split.1 = (bf16[16,512]{1,0:T(8,128)(2,1)}, bf16[16,128]{1,0:T(8,128)(2,1)}, bf16[16,128]{1,0:T(8,128)(2,1)}) custom-call(bf16[16,768]{1,0:T(8,128)(2,1)} %layer.1.both), custom_call_target="tpu_custom_call" | custom-call | tf_op jit(solution)/shard_map/split/pallas_call | solution.py:810

commit v6 on v5

--- a/solution.py
+++ b/solution.py
@@ -246,7 +246,8 @@
     for copy in locals_:
         copy.start()
 
-    inputs[2].wait()
+    for copy in inputs:
+        copy.wait()
 
     pl.semaphore_wait(barrier, NJ + NZ + NT - 3)
 
@@ -263,8 +264,6 @@
         )
 
     c_wa = chunk_of(wq_in, wq, 0, 0, 256)
-    for copy in inputs[0:2]:
-        copy.wait()
     tok = tokens[...].astype(F32)
     normed = (
         tok * lax.rsqrt(jnp.mean(tok * tok, axis=-1, keepdims=True) + norm_eps) * attn_gain[...]
@@ -289,8 +288,6 @@
         ),
     )
     c_wb = chunk_of(wq_in, wq, 1, 256, 512)
-    for copy in inputs[3:]:
-        copy.wait()
     c_wk = chunk_of(wk_in, wk, 2, 0, 128)
     c_wv = chunk_of(wv_in, wv, 9, 0, 128)
     c_wo = exchange(
@@ -663,14 +660,12 @@
     final = tokens[:, own_cols].astype(F32) + jnp.concatenate(
         [mixed[quarter, 2 * mt, own_rows], mixed[quarter, 2 * mt + 1, own_rows]], axis=1
     ).astype(F32)
-    for copy in started[: -len(c_f)]:
-        copy.wait_send()
     arrived(c_f)
     for z in range(NZ):
         final = final + fin_recv[z].astype(F32)
     out[:, 0:512] = final.astype(BF)
 
-    for copy in c_f:
+    for copy in started:
         copy.wait_send()
 
 

time: 74.9 us -> 74.6 us (level)
  no operation moved by 1% of the time
where the time goes in v6:
time: 74.6 us; the launch traced here: 74.4 us
  Pallas kernels  73.8 us (99%)
    pallas_call x1, Pallas kernels, body(): pl.pallas_call(kernel, name='layer', out_shape=jax.ShapeDtypeStruct((16,...  72.4 us

profile of v6, /device:TPU:1, one launch (start us, length us, event | category | flops | bytes accessed | tf_op | source)
XLA Modules:
  0.0 74.4 jit_solution(8343757129476557558)
XLA Ops:
  0.6 72.4 %layer.1.both = bf16[16,768]{1,0:T(8,128)(2,1)} custom-call(bf16[16,2048]{1,0:T(8,128)(2,1)} %tokens_in.1, f32[1,2048]{1,0:T(1,128)} %bitcast.7, bf16[32,512]{1,0:T(8,128)(2,1)} %wq_hbm.1, bf16[32,128]{1,0:T(8,128)(2,1)} %wk_hbm.1, bf16[32,128]{1,0:T(8,128)(2,1)} %wv_hbm.1, f32[4]{0:T(128)} %bias_hbm.1, bf16[16,1,1024,128]{3,2,1,0:T(8,128)(2,1)} %keys_hbm.1, ...), custom_call_target="tpu_custom_call" | custom-call | tf_op jit(solution)/shard_map/layer/pallas_call | solution.py:704
  73.1 1.4 %split.1 = (bf16[16,512]{1,0:T(8,128)(2,1)}, bf16[16,128]{1,0:T(8,128)(2,1)}, bf16[16,128]{1,0:T(8,128)(2,1)}) custom-call(bf16[16,768]{1,0:T(8,128)(2,1)} %layer.1.both), custom_call_target="tpu_custom_call" | custom-call | tf_op jit(solution)/shard_map/split/pallas_call | solution.py:805
